TPU v7x, 32 devices: a whole 2x2x4 slice. The times are simulated.
32 devices in a mesh: fs: 32 (over z, y, x, core), tp: 1.
Axes of the slice: x: 2, y: 2, z: 4, core: 2. Of those that a mesh axis runs over, the one named last changes fastest.
Arguments:
- later_input: bfloat16 [6144, 2048], P(('fs', 'tp')), may hold values from -6 to 6
- earlier_input: bfloat16 [6144, 2048], P(('fs', 'tp')), may hold values from -6 to 6
- cotangent: bfloat16 [6144, 2048], P(('fs', 'tp')), may hold values from -6 to 6
- gate_weight: bfloat16 [2048, 3072], P('fs', 'tp'), may hold values from -0.125 to 0.125
- up_weight: bfloat16 [2048, 3072], P('fs', 'tp'), may hold values from -0.125 to 0.125
- down_weight: bfloat16 [2048, 3072], P('fs', 'tp'), may hold values from -0.109375 to 0.109375
- down_grad_sum: float32 [2048, 3072], P('fs', 'tp'), may hold values from -6 to 6
Outputs:
- later_output: bfloat16 [6144, 2048], P(('fs', 'tp'))
- earlier_grad_input: bfloat16 [6144, 2048], P(('fs', 'tp'))
- new_down_grad_sum: float32 [2048, 3072], P('fs', 'tp')
All inputs are finite; a program needn't handle non-finite values.
Results may differ from a plain program's by a relative error of at most 0.0057.
Values may be sent and summed in bfloat16 or wider, within the bound.
A program may use at most 192 MiB of HBM per device.

v0:
```python
import functools

import jax
import jax.numpy as jnp
from jax import lax
from jax.experimental import pallas as pl
from jax.experimental.pallas import tpu as pltpu
from jax.sharding import PartitionSpec as P

QUAD = 4


def contract_last(leading, trailing):
    return lax.dot_general(
        leading, trailing, (((1,), (1,)), ((), ())), preferred_element_type=jnp.float32
    )


def add_parts(received, group):
    pieces = received.reshape(group, received.shape[0] // group, received.shape[1])
    return jnp.sum(pieces.astype(jnp.float32), axis=0).astype(jnp.bfloat16)


def shards(
    later_input, earlier_input, cotangent, gate_weight, up_weight, down_weight, down_grad_sum
):
    group = lax.axis_size("tp")
    later_rows, early_rows, grad_rows = (
        lax.all_gather(later_input, "tp", axis=0, tiled=True),
        lax.all_gather(earlier_input, "tp", axis=0, tiled=True),
        lax.all_gather(cotangent, "tp", axis=0, tiled=True),
    )
    columns = later_rows
    gate_later = jnp.dot(
        columns,
        lax.all_gather(gate_weight, "fs", axis=0, tiled=True),
        preferred_element_type=jnp.float32,
    )
    up_later = jnp.dot(
        columns,
        lax.all_gather(up_weight, "fs", axis=0, tiled=True),
        preferred_element_type=jnp.float32,
    )
    hidden_later = (jax.nn.silu(gate_later) * up_later).astype(jnp.bfloat16)
    partials = contract_last(hidden_later, lax.all_gather(down_weight, "fs", axis=0, tiled=True))
    gate_whole, up_whole, down_whole = (
        lax.all_gather(gate_weight, "fs", axis=0, tiled=True),
        lax.all_gather(up_weight, "fs", axis=0, tiled=True),
        lax.all_gather(down_weight, "fs", axis=0, tiled=True),
    )
    output_received = lax.all_to_all(
        partials.astype(jnp.bfloat16), "tp", split_axis=0, concat_axis=0, tiled=True
    )
    later_output = add_parts(output_received, group)
    gate_early = jnp.dot(early_rows, gate_whole, preferred_element_type=jnp.float32)
    up_early = jnp.dot(early_rows, up_whole, preferred_element_type=jnp.float32)
    sigmoid_gate = jax.nn.sigmoid(gate_early)
    activated = gate_early * sigmoid_gate
    hidden_early = (activated * up_early).astype(jnp.bfloat16)
    grad_hidden = jnp.dot(grad_rows, down_whole, preferred_element_type=jnp.float32)
    grad_gate = (
        grad_hidden * up_early * sigmoid_gate * (1.0 + gate_early * (1.0 - sigmoid_gate))
    ).astype(jnp.bfloat16)
    grad_up = (grad_hidden * activated).astype(jnp.bfloat16)
    input_partial = contract_last(grad_gate, gate_whole) + contract_last(grad_up, up_whole)
    input_received = lax.all_to_all(
        input_partial.astype(jnp.bfloat16), "tp", split_axis=0, concat_axis=0, tiled=True
    )
    earlier_grad_input = add_parts(input_received, group)
    columns = grad_rows
    summed = lax.psum_scatter(
        lax.dot_general(
            columns, hidden_early, (((0,), (0,)), ((), ())), preferred_element_type=jnp.float32
        ),
        "fs",
        scatter_dimension=0,
        tiled=True,
    )
    factor = (later_rows.shape[0] * lax.axis_size("fs")) ** (-0.5)
    return (later_output, earlier_grad_input, down_grad_sum + summed * factor)

def quads_of(total):
    return [[first + place for place in range(QUAD)] for first in range(0, total, QUAD)]


def lanes_of(total):
    return [[first + place for first in range(0, total, QUAD)] for place in range(QUAD)]


def swap(value, bit):
    total = lax.axis_size("fs")
    return lax.ppermute(value, "fs", [(index, index ^ bit) for index in range(total)])


def return_tokens(partial):
    blocks = partial.astype(jnp.bfloat16).reshape(QUAD, -1, partial.shape[1])
    mine = partial.reshape(blocks.shape)
    near = swap(jnp.stack([blocks[1], blocks[3]]), 1).astype(jnp.float32)
    far = swap((mine[2] + near[1]).astype(jnp.bfloat16), 2)
    return (mine[0] + near[0] + far.astype(jnp.float32)).astype(jnp.bfloat16)

def ring_group(place, ring):
    half = lax.div(2 * place, ring)
    return 2 * place * (1 - half) + (2 * (ring - 1 - place) + 1) * half


def ring_place(group, ring):
    odd = lax.rem(group, 2)
    return lax.div(group, 2) * (1 - odd) + (ring - 1 - lax.div(group, 2)) * odd


def gather_kernel(ring, weights, tokens, *refs):
    weight_refs, token_refs = refs[:weights], refs[weights : weights + tokens]
    outs = refs[weights + tokens : 2 * (weights + tokens)]
    whole_refs, rows_refs = outs[:weights], outs[weights:]
    ring_send, ring_recv, quad_send, quad_recv, token_send, token_recv, local_sem = refs[
        2 * (weights + tokens) :
    ]
    me = lax.axis_index("fs")
    group, lane = lax.div(me, QUAD), lax.rem(me, QUAD)
    low, high = lax.rem(lane, 2), lax.div(lane, 2)
    relative = [lane, lane + 1 - 2 * low, lane + 2 - 4 * high, QUAD - 1 - lane]
    peers = [group * QUAD + other for other in relative]
    place = ring_place(group, ring)
    around = [
        ring_group(lax.rem(place + shift, ring), ring) * QUAD + lane for shift in (1, ring - 1)
    ]
    depth = weight_refs[0].shape[0]
    width = weight_refs[0].shape[1] // QUAD

    barrier = pltpu.get_barrier_semaphore()
    for other in peers[1:] + around:
        pl.semaphore_signal(
            barrier, inc=1, device_id={"fs": other}, device_id_type=pl.DeviceIdType.MESH
        )
    pl.semaphore_wait(barrier, QUAD + 1)

    def remote(source, target, send, recv, other):
        return pltpu.make_async_remote_copy(
            src_ref=source,
            dst_ref=target,
            send_sem=send,
            recv_sem=recv,
            device_id={"fs": other},
            device_id_type=pl.DeviceIdType.MESH,
        )

    def slab(weight, owner, member):
        first = pl.multiple_of((owner * QUAD + member) * depth, depth)
        return whole_refs[weight].at[pl.ds(first, depth), :]

    def columns(weight, member):
        return weight_refs[weight].at[:, pl.ds(pl.multiple_of(member * width, width), width)]

    sent, kept = [], []
    quad, hops, rows = {}, {}, {}
    for weight in range(weights):
        for far in (3, 2, 1):
            copy = remote(
                columns(weight, relative[far]),
                slab(weight, group, lane),
                quad_send.at[weight, far - 1],
                quad_recv.at[weight, far - 1],
                peers[far],
            )
            copy.start()
            quad[weight, far] = copy
            sent.append(copy)
    for weight in range(weights):
        copy = pltpu.make_async_copy(
            columns(weight, lane), slab(weight, group, lane), local_sem.at[weight]
        )
        copy.start()
        kept.append(copy)

    def row_block(token, block):
        count = token_refs[token].shape[0]
        return rows_refs[token].at[pl.ds(block * count, count), :]

    def send_rows(token, source, block, slot, other):
        copy = remote(
            source,
            row_block(token, block),
            token_send.at[token, slot],
            token_recv.at[token, slot],
            other,
        )
        copy.start()
        rows[token, slot] = copy
        sent.append(copy)

    for token in range(tokens):
        send_rows(token, token_refs[token], 2, 1, peers[2])
    for token in range(tokens):
        send_rows(token, token_refs[token], 1, 0, peers[1])
        copy = pltpu.make_async_copy(
            token_refs[token], row_block(token, 0), local_sem.at[weights + token]
        )
        copy.start()
        kept.append(copy)

    for step in range(ring - 1):
        for weight in range(weights):
            for piece in (0, 1, 3, 2):
                if step:
                    hops[weight, piece, step - 1].wait_recv()
                elif piece:
                    quad[weight, piece].wait_recv()
                forward = piece in (0, 3)
                back = ring - step if forward else step
                owner = ring_group(lax.rem(place + back, ring), ring)
                target = slab(weight, owner, relative[piece])
                copy = remote(
                    columns(weight, lane) if step == 0 and piece == 0 else target,
                    target,
                    ring_send.at[weight, piece, step],
                    ring_recv.at[weight, piece, step],
                    around[0 if forward else 1],
                )
                copy.start()
                hops[weight, piece, step] = copy
                sent.append(copy)
        for token in range(tokens):
            if step == ring - 2 - 2 * (tokens - 1 - token):
                rows[token, 1].wait_recv()
                send_rows(token, row_block(token, 2), 3, 2, peers[1])
    for weight in range(weights):
        for piece in range(QUAD):
            hops[weight, piece, ring - 2].wait_recv()
    for token in range(tokens):
        rows[token, 0].wait_recv()
        rows[token, 2].wait_recv()
    for copy in sent:
        copy.wait_send()
    for copy in kept:
        copy.wait()


def gather(identity, weight_list, token_list):
    ring = lax.axis_size("fs") // QUAD
    weights, tokens = len(weight_list), len(token_list)
    dma = pltpu.SemaphoreType.DMA
    outs = [
        jax.ShapeDtypeStruct((w.shape[0] * QUAD * ring, w.shape[1] // QUAD), w.dtype)
        for w in weight_list
    ] + [jax.ShapeDtypeStruct((t.shape[0] * QUAD, t.shape[1]), t.dtype) for t in token_list]
    return pl.pallas_call(
        functools.partial(gather_kernel, ring, weights, tokens),
        out_shape=outs,
        in_specs=[pl.BlockSpec(memory_space=pltpu.VMEM)] * (weights + tokens),
        out_specs=[pl.BlockSpec(memory_space=pl.ANY)] * (weights + tokens),
        scratch_shapes=[
            dma((weights, QUAD, ring - 1)),
            dma((weights, QUAD, ring - 1)),
            dma((weights, QUAD - 1)),
            dma((weights, QUAD - 1)),
            dma((tokens, 3)),
            dma((tokens, 3)),
            dma((weights + tokens,)),
        ],
        compiler_params=pltpu.CompilerParams(collective_id=identity, has_side_effects=True),
        cost_estimate=pl.CostEstimate(
            flops=0, bytes_accessed=weights * 90_000_000, transcendentals=0
        ),
    )(*weight_list, *token_list)


def quad_shards(
    later_input, earlier_input, cotangent, gate_weight, up_weight, down_weight, down_grad_sum
):
    total = lax.axis_size("fs")
    gate_whole, up_whole, down_whole, early_rows, grad_rows, later_rows = gather(
        0, (gate_weight, up_weight, down_weight), (earlier_input, cotangent, later_input)
    )

    gate_early = jnp.dot(early_rows, gate_whole, preferred_element_type=jnp.float32)
    up_early = jnp.dot(early_rows, up_whole, preferred_element_type=jnp.float32)
    sigmoid_gate = jax.nn.sigmoid(gate_early)
    activated = gate_early * sigmoid_gate
    hidden_early = (activated * up_early).astype(jnp.bfloat16)
    partial_sum = lax.dot_general(
        grad_rows, hidden_early, (((0,), (0,)), ((), ())), preferred_element_type=jnp.float32
    ).astype(jnp.bfloat16)
    summed = lax.psum_scatter(
        partial_sum,
        "fs",
        scatter_dimension=0,
        tiled=True,
        axis_index_groups=lanes_of(total),
    )
    down_whole, later_rows, _ = lax.optimization_barrier(
        (down_whole, later_rows, partial_sum)
    )
    gate_later = jnp.dot(later_rows, gate_whole, preferred_element_type=jnp.float32)
    up_later = jnp.dot(later_rows, up_whole, preferred_element_type=jnp.float32)
    hidden_later = (jax.nn.silu(gate_later) * up_later).astype(jnp.bfloat16)

    grad_hidden = jnp.dot(grad_rows, down_whole, preferred_element_type=jnp.float32)
    grad_gate = (
        grad_hidden * up_early * sigmoid_gate * (1.0 + gate_early * (1.0 - sigmoid_gate))
    ).astype(jnp.bfloat16)
    grad_up = (grad_hidden * activated).astype(jnp.bfloat16)
    later_output = return_tokens(contract_last(hidden_later, down_whole))
    earlier_grad_input = return_tokens(
        contract_last(grad_gate, gate_whole) + contract_last(grad_up, up_whole)
    )
    own_rows = lax.all_to_all(
        summed, "fs", split_axis=0, concat_axis=1, tiled=True, axis_index_groups=quads_of(total)
    )
    factor = (later_input.shape[0] * total) ** (-0.5)
    return (
        later_output,
        earlier_grad_input,
        down_grad_sum + own_rows.astype(jnp.float32) * factor,
    )


def solution(mesh):
    in_specs = (
        P(("fs", "tp"), None),
        P(("fs", "tp"), None),
        P(("fs", "tp"), None),
        P("fs", "tp"),
        P("fs", "tp"),
        P("fs", "tp"),
        P("fs", "tp"),
    )
    out_specs = (P(("fs", "tp"), None), P(("fs", "tp"), None), P("fs", "tp"))
    split = mesh.shape["tp"] == 1 and mesh.shape["fs"] % (2 * QUAD) == 0
    body = quad_shards if split else shards
    return jax.shard_map(body, mesh=mesh, in_specs=in_specs, out_specs=out_specs, check_vma=False)
```

profile of v0, /device:TPU:0, one launch (start us, length us, event | category | flops | bytes accessed | tf_op | source)
XLA Modules:
  0.0 216.4 jit_solution(6152215082142050151)
XLA Ops:
  7.2 0.0 reduce-scatter.2.cloned.1.call-start
  7.2 102.1 %shard_map.94 = (bf16[2048,768]{1,0:T(8,128)(2,1)}, bf16[2048,768]{1,0:T(8,128)(2,1)}, bf16[2048,768]{1,0:T(8,128)(2,1)}, bf16[768,2048]{1,0:T(8,128)(2,1)}, bf1...) custom-call(bf16[64,3072]{1,0:T(8,128)(2,1)} %refs_0_.1, bf16[64,3072]{1,0:T(8,128)(2,1)} %refs_1_.1, ...), custom_call_target="tpu_custom_call" | custom-call | bytes 270000000 | tf_op jit(solution)/shard_map/pallas_call | solution.py:247
  109.3 0.0 copy-start
  109.4 0.0 copy-start.7
  109.4 5.6 %fusion.22 = f32[768,768]{1,0:T(8,128)S(1)} fusion(bf16[768,2048]{1,0:T(8,128)(2,1)} %get-tuple-element.14, bf16[2048,768]{1,0:T(8,128)(2,1)} %get-tuple-element.15), kind=kOutput, calls=%fused_computation.38 | convolution fusion | flops 2415919104 | bytes 8650752 | tf_op jit(solution)/shard_map/dot_general | solution.py:276
  114.9 0.0 copy-start.1
  115.0 0.0 copy-done
  115.0 0.0 copy-done.7
  115.0 0.0 copy-start.6
  115.0 2.6 %fusion.23 = f32[768,768]{1,0:T(8,128)S(1)} fusion(bf16[768,2048]{1,0:T(8,128)(2,1)S(1)} %copy-done.7, bf16[2048,768]{1,0:T(8,128)(2,1)S(1)} %copy-done), kind=kOutput, calls=%fused_computation.39 | convolution fusion | flops 2415919104 | bytes 8650752 | tf_op jit(solution)/shard_map/dot_general | solution.py:277
  117.6 0.0 copy-start.8
  117.6 0.0 copy-done.1
  117.6 1.5 copy-done.8
  119.1 0.0 copy-done.6
  119.1 4.4 %convolution_convert_fusion = bf16[2048,768]{1,0:T(8,128)(2,1)} fusion(bf16[768,2048]{1,0:T(8,128)(2,1)S(1)} %copy-done.6, f32[768,768]{1,0:T(8,128)S(1)} %fusion.23, f32[768,768]{1,0:T(8,128)S(1)} %fusion.22), kind=kOutput, calls=%fused_computation.1 | convolution fusion | flops 2421030912 | bytes 11010048 | tf_op jit(solution)/shard_map/dot_general | solution.py:281
  123.5 0.0 reduce-scatter.2.cloned.1.call-update
  123.6 0.0 copy-start.2
  123.6 0.0 copy-start.5
  123.6 5.6 %fusion.25 = f32[768,768]{1,0:T(8,128)S(1)} fusion(bf16[768,2048]{1,0:T(8,128)(2,1)} %get-tuple-element.13, bf16[2048,768]{1,0:T(8,128)(2,1)} %get-tuple-element.18), kind=kOutput, calls=%fused_computation.41 | convolution fusion | flops 2415919104 | bytes 8650752 | tf_op jit(solution)/shard_map/dot_general | solution.py:298
  129.2 3.3 %fusion.11 = f32[768,2048]{1,0:T(8,128)S(1)} fusion(bf16[2048,768]{1,0:T(8,128)(2,1)S(1)} %copy-done.5, f32[768,768]{1,0:T(8,128)S(1)} %copy-done.2, f32[768,768]{1,0:T(8,128)S(1)} %fusion.25, f32[768,768]{1,0:T(8,128)S(1)} %copy-done.9), kind=kOutput, calls=%fused_computation.24 | convolution fusion | flops 2421817344 | bytes 16515072 | tf_op jit(solution)/shard_map/dot_general | solution.py:14
  132.5 4.5 %fusion.21 = (bf16[768,2048]{1,0:T(8,128)(2,1)S(1)}, f32[768,2048]{1,0:T(8,128)}) fusion(f32[768,2048]{1,0:T(8,128)S(1)} %fusion.11, bf16[2048,768]{1,0:T(8,128)(2,1)S(1)} %copy-done, f32[768,768]{1,0:T(8,128)S(1)} %fusion.25, f32[768,768]{1,0:T(8,128)S(1)} %copy-done.2), kind=kOutput, calls=%fused_computation.37 | convolution fusion | flops 2422603776 | bytes 23592960 | tf_op jit(solution)/shard_map/dot_general | solution.py:14
  137.0 0.2 slice_bitcast_fusion.5
  137.2 1.3 pad_maximum_fusion.1
  138.5 0.0 collective-permute-start.2
  138.5 1.2 copy-done.4
  139.6 4.1 %fusion.24 = f32[768,768]{1,0:T(8,128)} fusion(bf16[768,2048]{1,0:T(8,128)(2,1)S(1)} %copy-done.4, bf16[2048,768]{1,0:T(8,128)(2,1)S(1)} %copy-done.5), kind=kOutput, calls=%fused_computation.40 | convolution fusion | flops 2415919104 | bytes 8650752 | tf_op jit(solution)/shard_map/dot_general | solution.py:294
  143.8 11.2 %fusion.20 = (bf16[768,2048]{1,0:T(8,128)(2,1)}, f32[768,2048]{1,0:T(8,128)}) fusion(bf16[2048,768]{1,0:T(8,128)(2,1)} %get-tuple-element.18, f32[768,768]{1,0:T(8,128)} %fusion.24, bf16[768,2048]{1,0:T(8,128)(2,1)} %get-tuple-element.17, bf16[2048,768]{1,0:T(8,128)(2,1)S(1)} %copy-done), kind=kOutput, calls=%fused_computation.36 | convolution fusion | flops 4836950016 | bytes 21233664 | tf_op jit(solution)/shard_map/dot_general | solution.py:14
  154.9 1.5 slice_bitcast_fusion.7
  156.4 0.1 pad_maximum_fusion
  156.6 0.1 collective-permute-start
  156.7 0.0 collective-permute-done.2
  156.7 1.8 convert_element_type.61
  158.5 1.7 fusion.2
  160.1 0.8 collective-permute-start.3
  160.9 0.0 collective-permute-done
  160.9 0.4 convert_element_type.54
  161.3 2.5 %fusion.7 = bf16[192,2048]{1,0:T(8,128)(2,1)} fusion(f32[2,192,2048]{2,1,0:T(8,128)S(1)} %convert_element_type.54, f32[768,2048]{1,0:T(8,128)} %get-tuple-element.24), kind=kLoop, calls=%fused_computation.17 | loop fusion | flops 786432 | bytes 3932160 | tf_op jit(solution)/shard_map/convert_element_type | solution.py:99
  163.8 1.3 collective-permute-start.1
  165.1 15.5 %collective-permute-done.3 = bf16[192,2048]{1,0:T(8,128)(2,1)S(1)} collective-permute-done((bf16[192,2048]{1,0:T(8,128)(2,1)S(1)}, bf16[192,2048]{1,0:T(8,128)(2,1)S(1)}, u32[]{:S(2)}, u32[]{:S(2)}) %collective-permute-start.3) | collective-permute-done | bytes 786464 | tf_op jit(solution)/shard_map/ppermute | solution.py:92
  180.6 2.7 %fusion.5 = bf16[192,2048]{1,0:T(8,128)(2,1)} fusion(f32[2,192,2048]{2,1,0:T(8,128)S(1)} %convert_element_type.61, f32[768,2048]{1,0:T(8,128)} %get-tuple-element.26, bf16[192,2048]{1,0:T(8,128)(2,1)S(1)} %collective-permute-done.3), kind=kLoop, calls=%fused_computation.14 | loop fusion | flops 1572864 | bytes 4718592 | tf_op jit(solution)/shard_map/convert_element_type | solution.py:100
  183.3 14.3 %reduce-scatter.2.cloned.1.call-done = bf16[256,768]{1,0:T(8,128)(2,1)} async-done(((bf16[2048,768]{1,0:T(8,128)(2,1)}), bf16[256,768]{1,0:T(8,128)(2,1)}) %reduce-scatter.2.cloned.1.call-update) | async-done | bytes 393232 | tf_op jit(solution)/shard_map/reduce_scatter | solution.py:284
  197.6 3.5 %all-to-all-start = ((bf16[4,64,768]{2,1,0:T(8,128)(2,1)}), bf16[4,64,768]{2,1,0:T(8,128)(2,1)S(1)}, u32[]{:S(2)}, u32[]{:S(2)}) async-start(bf16[4,64,768]{2,1,0:T(8,128)(2,1)} %bitcast.56), calls=%async_computation.1 | async-start | bytes 786432 | tf_op jit(solution)/shard_map/all_to_all | solution.py:307
  201.0 0.0 collective-permute-done.1
  201.1 2.8 %fusion.10 = bf16[192,2048]{1,0:T(8,128)(2,1)} fusion(f32[2,192,2048]{2,1,0:T(8,128)S(1)} %convert_element_type.54, f32[768,2048]{1,0:T(8,128)} %get-tuple-element.24, bf16[192,2048]{1,0:T(8,128)(2,1)} %collective-permute-done.1), kind=kLoop, calls=%fused_computation.21 | loop fusion | flops 1572864 | bytes 4718592 | tf_op jit(solution)/shard_map/convert_element_type | solution.py:100
  203.9 4.6 %all-to-all-done = bf16[4,64,768]{2,1,0:T(8,128)(2,1)S(1)} async-done(((bf16[4,64,768]{2,1,0:T(8,128)(2,1)}), bf16[4,64,768]{2,1,0:T(8,128)(2,1)S(1)}, u32[]{:S(2)}, u32[]{:S(2)}) %all-to-all-start) | async-done | bytes 393248 | tf_op jit(solution)/shard_map/all_to_all | solution.py:307
  208.4 0.1 multiply_bitcast_fusion
  208.5 0.1 copy.11
  208.6 1.0 add.46
  (7 shorter events, 0.0 us)
Async XLA Ops:
  7.2 190.4 %reduce-scatter.2.cloned.1.call-start = ((), (), s32[]{:S(2)}) async-start(), calls=%async_computation.2 | async-start | bytes 3538944 | tf_op jit(solution)/shard_map/reduce_scatter | solution.py:284
  109.3 5.6 %copy-start = (bf16[2048,768]{1,0:T(8,128)(2,1)S(1)}, bf16[2048,768]{1,0:T(8,128)(2,1)}, u32[]{:S(2)}) copy-start(bf16[2048,768]{1,0:T(8,128)(2,1)} %get-tuple-element.16) | copy-start | bytes 9437188
  109.4 5.6 %copy-start.7 = (bf16[768,2048]{1,0:T(8,128)(2,1)S(1)}, bf16[768,2048]{1,0:T(8,128)(2,1)}, u32[]{:S(2)}) copy-start(bf16[768,2048]{1,0:T(8,128)(2,1)} %get-tuple-element.14) | copy-start | bytes 9437188
  114.9 2.7 %copy-start.1 = (f32[768,768]{1,0:T(8,128)}, f32[768,768]{1,0:T(8,128)S(1)}, u32[]{:S(2)}) copy-start(f32[768,768]{1,0:T(8,128)S(1)} %fusion.22) | copy-start | bytes 7077892
  115.0 4.1 %copy-start.6 = (bf16[768,2048]{1,0:T(8,128)(2,1)S(1)}, bf16[768,2048]{1,0:T(8,128)(2,1)}, u32[]{:S(2)}) copy-start(bf16[768,2048]{1,0:T(8,128)(2,1)} %get-tuple-element.13) | copy-start | bytes 9437188
  117.6 1.5 copy-start.8
  123.6 5.6 %copy-start.2 = (f32[768,768]{1,0:T(8,128)S(1)}, f32[768,768]{1,0:T(8,128)}, u32[]{:S(2)}) copy-start(f32[768,768]{1,0:T(8,128)} %copy-done.1) | copy-start | bytes 7077892
  123.6 5.6 %copy-start.5 = (bf16[2048,768]{1,0:T(8,128)(2,1)S(1)}, bf16[2048,768]{1,0:T(8,128)(2,1)}, u32[]{:S(2)}) copy-start(bf16[2048,768]{1,0:T(8,128)(2,1)} %get-tuple-element.15) | copy-start | bytes 9437188
  123.6 5.6 %copy-start.9 = (f32[768,768]{1,0:T(8,128)S(1)}, f32[768,768]{1,0:T(8,128)}, u32[]{:S(2)}) copy-start(f32[768,768]{1,0:T(8,128)} %copy-done.8) | copy-start | bytes 7077892
  137.2 2.5 %copy-start.4 = (bf16[768,2048]{1,0:T(8,128)(2,1)S(1)}, bf16[768,2048]{1,0:T(8,128)(2,1)}, u32[]{:S(2)}) copy-start(bf16[768,2048]{1,0:T(8,128)(2,1)} %get-tuple-element.17) | copy-start | bytes 9437188
  138.5 18.2 %collective-permute-start.2 = (bf16[2,192,2048]{2,1,0:T(8,128)(2,1)}, bf16[2,192,2048]{2,1,0:T(8,128)(2,1)}, u32[]{:S(2)}, u32[]{:S(2)}) collective-permute-start(bf16[2,192,2048]{2,1,0:T(8,128)(2,1)} %pad_maximum_fusion.1), channel_id=1, source_target_pairs={{0,1},{1,0},{2,3},{3,2},{4,5},{5,4},{6,7},{7,6},{8,9},{9,8},{10,11... | collective-permute-start | bytes 4718600 | tf_op jit(solution)/shard_map/ppermute | solution.py:92
  156.6 4.3 %collective-permute-start = (bf16[2,192,2048]{2,1,0:T(8,128)(2,1)S(1)}, bf16[2,192,2048]{2,1,0:T(8,128)(2,1)S(1)}, u32[]{:S(2)}, u32[]{:S(2)}) collective-permute-start(bf16[2,192,2048]{2,1,0:T(8,128)(2,1)S(1)} %pad_maximum_fusion), channel_id=1, source_target_pairs={{0,1},{1,0},{2,3},{3,2},{4,5},{5,4},{6,7},{7,6},{8,9},{9,8},{10,11... | collective-permute-start | bytes 4718600 | tf_op jit(solution)/shard_map/ppermute | solution.py:92
  160.1 20.5 %collective-permute-start.3 = (bf16[192,2048]{1,0:T(8,128)(2,1)S(1)}, bf16[192,2048]{1,0:T(8,128)(2,1)S(1)}, u32[]{:S(2)}, u32[]{:S(2)}) collective-permute-start(bf16[192,2048]{1,0:T(8,128)(2,1)S(1)} %fusion.2), channel_id=1, source_target_pairs={{0,2},{1,3},{2,0},{3,1},{4,6},{5,7},{6,4},{7,5},{8,10},{9,11},{10,... | collective-permute-start | bytes 2359304 | tf_op jit(solution)/shard_map/ppermute | solution.py:92
  163.8 37.3 %collective-permute-start.1 = (bf16[192,2048]{1,0:T(8,128)(2,1)}, bf16[192,2048]{1,0:T(8,128)(2,1)}, u32[]{:S(2)}, u32[]{:S(2)}) collective-permute-start(bf16[192,2048]{1,0:T(8,128)(2,1)} %fusion.7), channel_id=1, source_target_pairs={{0,2},{1,3},{2,0},{3,1},{4,6},{5,7},{6,4},{7,5},{8,10},{9,11},{10,... | collective-permute-start | bytes 2359304 | tf_op jit(solution)/shard_map/ppermute | solution.py:92
  197.6 10.8 %all-to-all-start = ((bf16[4,64,768]{2,1,0:T(8,128)(2,1)}), bf16[4,64,768]{2,1,0:T(8,128)(2,1)S(1)}, u32[]{:S(2)}, u32[]{:S(2)}) async-start(bf16[4,64,768]{2,1,0:T(8,128)(2,1)} %bitcast.56), calls=%async_computation.1 | async-start | bytes 786432 | tf_op jit(solution)/shard_map/all_to_all | solution.py:307
  203.9 4.7 %copy-start.3 = (f32[64,3072]{1,0:T(8,128)S(1)}, f32[64,3072]{1,0:T(8,128)}, u32[]{:S(2)}) copy-start(f32[64,3072]{1,0:T(8,128)} %param.13) | copy-start | bytes 2359300
Sparse Core Ops, SparseCore 0:
  123.7 73.8 reduce-scatter.1
where the time goes:
time: 217 us; the launch traced here: 216 us
  Pallas kernels  102 us (47%)
  matrix products  41.3 us (19%)
  waiting for transfers between devices  34.4 us (16%)
  between operations  14.3 us (7%)
  other arithmetic  14.2 us (7%)
  starting transfers between devices  5.66 us (3%)
  local copies, waits for them, and re-layouts  4.39 us (2%)
    pallas_call x1, Pallas kernels, gather(): pl.pallas_call(functools.partial(gather_kernel, ring, weights, tokens), o...  102 us
    dot_general x3, matrix products, contract_last(): lax.dot_general(leading, trailing, (((1,), (1,)), ((), ())), preferred_el...  19 us
    ppermute x4, waiting for transfers between devices, swap(): lax.ppermute(value, 'fs', [(index, index ^ bit) for index in range(total)])  15.6 us
    reduce_scatter x1, waiting for transfers between devices, quad_shards(): lax.psum_scatter(partial_sum, 'fs', scatter_dimension=0, tiled=True, axis...  14.3 us
    dot_general x1, matrix products, quad_shards(): jnp.dot(grad_rows, down_whole, preferred_element_type=jnp.float32)  5.58 us
    dot_general x1, matrix products, quad_shards(): jnp.dot(early_rows, gate_whole, preferred_element_type=jnp.float32)  5.58 us
    convert_element_type x2, other arithmetic, return_tokens(): return (mine[0] + near[0] + far.astype(jnp.float32)).astype(jnp.bfloat16)  5.47 us
    all_to_all x1, waiting for transfers between devices, quad_shards(): lax.all_to_all(summed, 'fs', split_axis=0, concat_axis=1, tiled=True, axi...  4.55 us
  transfers between devices with their start and end apart: 6, of which 3 were waited for; matrix products, arithmetic and copies ran while one was open for 20% of the time, Pallas kernels for 0%

commit v1 on v0

v1 whole, which is shorter than its diff:
```python
import functools

import jax
import jax.numpy as jnp
from jax import lax
from jax.experimental import pallas as pl
from jax.experimental.pallas import tpu as pltpu
from jax.sharding import PartitionSpec as P

QUAD = 4


def contract_last(leading, trailing):
    return lax.dot_general(
        leading, trailing, (((1,), (1,)), ((), ())), preferred_element_type=jnp.float32
    )


def add_parts(received, group):
    pieces = received.reshape(group, received.shape[0] // group, received.shape[1])
    return jnp.sum(pieces.astype(jnp.float32), axis=0).astype(jnp.bfloat16)


def shards(
    later_input, earlier_input, cotangent, gate_weight, up_weight, down_weight, down_grad_sum
):
    group = lax.axis_size("tp")
    later_rows, early_rows, grad_rows = (
        lax.all_gather(later_input, "tp", axis=0, tiled=True),
        lax.all_gather(earlier_input, "tp", axis=0, tiled=True),
        lax.all_gather(cotangent, "tp", axis=0, tiled=True),
    )
    columns = later_rows
    gate_later = jnp.dot(
        columns,
        lax.all_gather(gate_weight, "fs", axis=0, tiled=True),
        preferred_element_type=jnp.float32,
    )
    up_later = jnp.dot(
        columns,
        lax.all_gather(up_weight, "fs", axis=0, tiled=True),
        preferred_element_type=jnp.float32,
    )
    hidden_later = (jax.nn.silu(gate_later) * up_later).astype(jnp.bfloat16)
    partials = contract_last(hidden_later, lax.all_gather(down_weight, "fs", axis=0, tiled=True))
    gate_whole, up_whole, down_whole = (
        lax.all_gather(gate_weight, "fs", axis=0, tiled=True),
        lax.all_gather(up_weight, "fs", axis=0, tiled=True),
        lax.all_gather(down_weight, "fs", axis=0, tiled=True),
    )
    output_received = lax.all_to_all(
        partials.astype(jnp.bfloat16), "tp", split_axis=0, concat_axis=0, tiled=True
    )
    later_output = add_parts(output_received, group)
    gate_early = jnp.dot(early_rows, gate_whole, preferred_element_type=jnp.float32)
    up_early = jnp.dot(early_rows, up_whole, preferred_element_type=jnp.float32)
    sigmoid_gate = jax.nn.sigmoid(gate_early)
    activated = gate_early * sigmoid_gate
    hidden_early = (activated * up_early).astype(jnp.bfloat16)
    grad_hidden = jnp.dot(grad_rows, down_whole, preferred_element_type=jnp.float32)
    grad_gate = (
        grad_hidden * up_early * sigmoid_gate * (1.0 + gate_early * (1.0 - sigmoid_gate))
    ).astype(jnp.bfloat16)
    grad_up = (grad_hidden * activated).astype(jnp.bfloat16)
    input_partial = contract_last(grad_gate, gate_whole) + contract_last(grad_up, up_whole)
    input_received = lax.all_to_all(
        input_partial.astype(jnp.bfloat16), "tp", split_axis=0, concat_axis=0, tiled=True
    )
    earlier_grad_input = add_parts(input_received, group)
    columns = grad_rows
    summed = lax.psum_scatter(
        lax.dot_general(
            columns, hidden_early, (((0,), (0,)), ((), ())), preferred_element_type=jnp.float32
        ),
        "fs",
        scatter_dimension=0,
        tiled=True,
    )
    factor = (later_rows.shape[0] * lax.axis_size("fs")) ** (-0.5)
    return (later_output, earlier_grad_input, down_grad_sum + summed * factor)

def ring_group(place, ring):
    half = lax.div(2 * place, ring)
    return 2 * place * (1 - half) + (2 * (ring - 1 - place) + 1) * half


def ring_place(group, ring):
    odd = lax.rem(group, 2)
    return lax.div(group, 2) * (1 - odd) + (ring - 1 - lax.div(group, 2)) * odd


def fused_kernel(ring, factor, *refs):
    token_refs, weight_refs, sum_ref = refs[:3], refs[3:6], refs[6]
    outs, sum_out = refs[7:9], refs[9]
    whole, tok, acc, mine, near_send, near_recv, far_send, far_recv, travel, trade_send, trade_recv = refs[10:21]
    (quad_ss, quad_rs, first_ss, first_rs, ring_ss, ring_rs, tok_ss, tok_rs, near_ss, near_rs,
     far_ss, far_rs, sum_ss, sum_rs, trade_ss, trade_rs, local_sem) = refs[21:]
    bf16, f32 = jnp.bfloat16, jnp.float32
    me = lax.axis_index("fs")
    group, lane = lax.div(me, QUAD), lax.rem(me, QUAD)
    low, high = lax.rem(lane, 2), lax.div(lane, 2)
    relative = [lane, lane + 1 - 2 * low, lane + 2 - 4 * high, QUAD - 1 - lane]
    peers = [group * QUAD + other for other in relative]
    place = ring_place(group, ring)

    def group_at(shift):
        return ring_group(lax.rem(place + shift + ring, ring), ring)

    around = [group_at(1) * QUAD + lane, group_at(-1) * QUAD + lane]
    depth = weight_refs[0].shape[0]
    width = whole.shape[2]
    chunk, half = QUAD * depth, 2 * depth
    rows = token_refs[0].shape[0]
    total_rows = tok.shape[1]
    reach = ring // 2
    per_slab = total_rows // chunk
    halves = [[high, 1 - high], [1 - high, high]]

    barrier = pltpu.get_barrier_semaphore()
    for other in peers[1:] + around:
        pl.semaphore_signal(
            barrier, inc=1, device_id={"fs": other}, device_id_type=pl.DeviceIdType.MESH
        )
    pl.semaphore_wait(barrier, QUAD + 1)

    def remote(source, target, send, recv, other):
        return pltpu.make_async_remote_copy(
            src_ref=source,
            dst_ref=target,
            send_sem=send,
            recv_sem=recv,
            device_id={"fs": other},
            device_id_type=pl.DeviceIdType.MESH,
        )

    def slab(weight, owner, member):
        first = pl.multiple_of((owner * QUAD + member) * depth, depth)
        return whole.at[weight, pl.ds(first, depth), :]

    def columns(weight, member):
        return weight_refs[weight].at[:, pl.ds(pl.multiple_of(member * width, width), width)]

    def half_slab(weight, owner, part):
        first = pl.multiple_of(owner * chunk + part * half, half)
        return whole.at[weight, pl.ds(first, half), :]

    sent, kept = [], []

    def begin(copy):
        copy.start()
        sent.append(copy)
        return copy

    quad, first_hop, hop, tokens = {}, {}, {}, {}
    for weight in range(3):
        for far in (1, 3, 2):
            quad[weight, far] = begin(
                remote(
                    columns(weight, relative[far]),
                    slab(weight, group, lane),
                    quad_ss.at[weight, far - 1],
                    quad_rs.at[weight, far - 1],
                    peers[far],
                )
            )

    def hop_first(weight, piece):
        for way in range(2):
            target = slab(weight, group, relative[piece])
            first_hop[weight, way, piece] = begin(
                remote(
                    columns(weight, lane) if piece == 0 else target,
                    target,
                    first_ss.at[weight, way, piece],
                    first_rs.at[weight, way, piece],
                    around[way],
                )
            )

    hop_first(0, 0)
    hop_first(1, 0)
    for weight in range(3):
        copy = pltpu.make_async_copy(
            columns(weight, lane), slab(weight, group, lane), local_sem.at[weight]
        )
        copy.start()
        kept.append(copy)

    def row_block(token, block):
        return tok.at[token, pl.ds(block * rows, rows), :]

    def send_rows(token, source, block, slot, other):
        tokens[token, slot] = begin(
            remote(
                source,
                row_block(token, block),
                tok_ss.at[token, slot],
                tok_rs.at[token, slot],
                other,
            )
        )

    for token in range(3):
        send_rows(token, token_refs[token], 2, 1, peers[2])
        send_rows(token, token_refs[token], 1, 0, peers[1])
        copy = pltpu.make_async_copy(
            token_refs[token], row_block(token, 0), local_sem.at[3 + token]
        )
        copy.start()
        kept.append(copy)

    def clear(index, carry):
        acc[index] = jnp.zeros(acc.shape[1:], f32)
        return carry

    lax.fori_loop(0, 4, clear, 0)
    acc[acc.shape[0] - 1] = jnp.zeros(acc.shape[1:], f32)

    for weight in (0, 1):
        quad[weight, 1].wait_recv()
        hop_first(weight, 1)
    hop_first(2, 0)
    quad[2, 1].wait_recv()
    hop_first(2, 1)
    for weight in range(3):
        for piece in (3, 2):
            quad[weight, piece].wait_recv()
            hop_first(weight, piece)
    for copy in kept:
        copy.wait()

    arrived = set()

    def arrival(weight, way, step, order):
        if (weight, way, step, order) in arrived:
            return
        arrived.add((weight, way, step, order))
        if step == 1:
            own_half = (order == 0) == (way == 0)
            for piece in (0, 1) if own_half else (3, 2):
                first_hop[weight, way, piece].wait_recv()
        else:
            hop[weight, way, step, order].wait_recv()

    def forward(weight, step, order):
        for way in range(2):
            arrival(weight, way, step - 1, order)
            shift = (1 - step) if way == 0 else (step - 1)
            part = half_slab(weight, group_at(shift), halves[way][order])
            hop[weight, way, step, order] = begin(
                remote(
                    part,
                    part,
                    ring_ss.at[weight, way, step - 2, order],
                    ring_rs.at[weight, way, step - 2, order],
                    around[way],
                )
            )

    def arrive(weight, distance):
        for way in range(2):
            for order in range(1 if distance == reach else 2):
                arrival(weight, way, distance, order)

    def token_over(token):
        tokens[token, 1].wait_recv()
        send_rows(token, row_block(token, 2), 3, 2, peers[1])

    def token_in(token):
        tokens[token, 0].wait_recv()
        tokens[token, 2].wait_recv()

    def span(owner):
        return pl.ds(pl.multiple_of(owner * chunk, chunk), chunk)

    def project(token, shift):
        where = span(group_at(shift))
        left = tok[token, :, where]
        for weight in range(2):
            slot = 2 * token + weight
            acc[slot] += jnp.dot(left, whole[weight, where, :], preferred_element_type=f32)

    def loop(first, last, body):
        def step(index, carry):
            body(index)
            return carry

        lax.fori_loop(first, last, step, 0)

    def project_pair(distance, token_list):
        if distance == reach:
            loop(0, len(token_list), lambda i: project(token_list[0] + i, reach))
        else:
            loop(
                0,
                2 * len(token_list),
                lambda i: project(
                    token_list[0] + lax.div(i, 2), (2 * lax.rem(i, 2) - 1) * distance
                ),
            )

    for order in range(2):
        for weight in (0, 1):
            forward(weight, 2, order)
    token_over(0)
    token_in(0)
    loop(0, 3, lambda i: project(0, i - 1))
    later_started = False
    for step in range(3, reach + 1):
        last = step == reach
        if last:
            token_over(1)
            token_in(1)
            loop(0, 3, lambda i: project(1, i - 1))
            for distance in range(2, reach - 1):
                project_pair(distance, [1])
        for order in range(1 if last else 2):
            for weight in (0, 1):
                forward(weight, step, order)
        if last:
            for order in range(2):
                forward(2, 2, order)
        for weight in (0, 1):
            arrive(weight, step - 1)
        project_pair(step - 1, [0, 1] if last else [0])
    token_over(2)
    for weight in (0, 1):
        arrive(weight, reach)
    project_pair(reach, [0, 1])
    for token in range(2):
        for slot in range(3):
            tokens[token, slot].wait_send()
            sent[:] = [copy for copy in sent if copy is not tokens[token, slot]]

    tile = 32

    def early_values(index):
        where = pl.ds(pl.multiple_of(index * tile, tile), tile)
        gate, up = acc[0, where, :], acc[1, where, :]
        sig = jax.nn.sigmoid(gate)
        act = gate * sig
        tok[0, where, 0:width] = (act * up).astype(bf16)
        acc[0, where, :] = up * sig * (1.0 + gate * (1.0 - sig))
        acc[1, where, :] = act

    def later_values(index):
        where = pl.ds(pl.multiple_of(index * tile, tile), tile)
        gate, up = acc[2, where, :], acc[3, where, :]
        tok[1, where, 0:width] = (gate * jax.nn.sigmoid(gate) * up).astype(bf16)

    loop(0, total_rows // tile, early_values)
    forward(2, 3, 0)
    loop(0, total_rows // tile, later_values)
    token_in(2)

    def slab_of(index):
        if isinstance(index, int):
            return 2 + index // per_slab, index % per_slab * chunk
        first = pl.multiple_of(lax.rem(index, per_slab) * chunk, chunk)
        return 2 + lax.div(index, per_slab), first

    def partial_sum(index):
        left = tok[2, :, span(group_at(index))]
        place_of, first = slab_of(index)
        acc[place_of, pl.ds(first, chunk), :] = lax.dot_general(
            left, tok[0, :, 0:width], (((0,), (0,)), ((), ())), preferred_element_type=f32
        )

    def own_part(shift, part):
        place_of, first = slab_of((shift + ring) % ring)
        return acc[place_of, pl.ds(pl.multiple_of(first + part * half, half), half), :]

    def near_copy(which, owner):
        return remote(
            near_send.at[which, owner],
            near_recv.at[which, owner],
            near_ss.at[which, owner],
            near_rs.at[which, owner],
            peers[1],
        )

    def far_copy(which, owner):
        return remote(
            far_send.at[which, owner],
            far_recv.at[which, owner],
            far_ss.at[which, owner],
            far_rs.at[which, owner],
            peers[2],
        )

    def produce(which, owner, value):
        mine[which, owner, 0] = value[:rows]
        mine[which, owner, 1] = value[2 * rows : 3 * rows]
        near_send[which, owner, 0] = value[rows : 2 * rows].astype(bf16)
        near_send[which, owner, 1] = value[3 * rows :].astype(bf16)
        near_copy(which, owner).start()

    def relay(which, owner):
        near_copy(which, owner).wait_recv()
        mine[which, owner, 0] += near_recv[which, owner, 0].astype(f32)
        far_send[which, owner] = (
            mine[which, owner, 1] + near_recv[which, owner, 1].astype(f32)
        ).astype(bf16)
        far_copy(which, owner).start()

    def finish(which, owner):
        far_copy(which, owner).wait_recv()
        outs[which][:, span(owner)] = (
            mine[which, owner, 0] + far_recv[which, owner].astype(f32)
        ).astype(bf16)

    last_slab = acc.shape[0] - 1

    def down_step(shift):
        owner = group_at(shift)
        where = span(owner)
        right = whole[2, where, :]
        produce(0, owner, contract_last(tok[1, :, 0:width], right))
        acc[last_slab] += jnp.dot(tok[2, :, where], right, preferred_element_type=f32)

    loop(0, 3, lambda i: down_step(i - 1))
    forward(2, 3, 1)
    loop(0, 3, lambda i: relay(0, group_at(i - 1)))
    loop(0, ring, partial_sum)

    for step in range(3, reach + 1):
        if step > 3:
            for order in range(1 if step == reach else 2):
                forward(2, step, order)
        arrive(2, step - 1)
        distance = step - 1
        loop(0, 2, lambda i: down_step((2 * i - 1) * distance))
        loop(0, 2, lambda i: relay(0, group_at((2 * i - 1) * distance)))

    moved = {}

    def pass_on(step, order, add):
        for way in range(2):
            part = halves[way][1 - order]
            shift = (reach + 1 - step) * (1 if way == 0 else -1)
            if add:
                moved[way, step - 1, order].wait_recv()
                travel[way, step - 1, order] = (
                    travel[way, step - 1, order].astype(f32) + own_part(shift, part)
                ).astype(bf16)
            else:
                travel[way, step - 1, order] = own_part(shift, part).astype(bf16)
        for way in range(2):
            moved[way, step, order] = begin(
                remote(
                    travel.at[way, step - 1, order],
                    travel.at[way, step, order],
                    sum_ss.at[way, step - 1, order],
                    sum_rs.at[way, step - 1, order],
                    around[way],
                )
            )

    pass_on(1, 1, False)
    pass_on(2, 0, False)
    arrive(2, reach)
    down_step(reach)

    def grads(index):
        where = pl.ds(pl.multiple_of(index * tile, tile), tile)
        hidden = acc[last_slab, where, :]
        tok[0, where, width : 2 * width] = (hidden * acc[0, where, :]).astype(bf16)
        tok[1, where, width : 2 * width] = (hidden * acc[1, where, :]).astype(bf16)

    loop(0, total_rows // tile, grads)
    relay(0, group_at(reach))

    def input_step(owner):
        where = span(owner)
        produce(
            1,
            owner,
            contract_last(tok[0, :, width : 2 * width], whole[0, where, :])
            + contract_last(tok[1, :, width : 2 * width], whole[1, where, :]),
        )

        @pl.when(owner > 0)
        def _():
            relay(1, owner - 1)

    pauses = [(2, 1)] + [(step, order) for step in range(3, reach + 1) for order in (0, 1)]
    stops = [ring // 4, ring // 2 + 1, ring]
    first = 0
    for stop in stops:
        loop(first, stop, input_step)
        first = stop
        if pauses:
            pass_on(*pauses.pop(0), True)
    relay(1, ring - 1)
    loop(0, ring, lambda i: finish(0, i))
    while pauses:
        pass_on(*pauses.pop(0), True)
    loop(0, ring, lambda i: finish(1, i))

    def total_of(part, order_pair):
        for way in range(2):
            moved[way, reach, order_pair[way]].wait_recv()
        return (
            own_part(0, part)
            + travel[0, reach, order_pair[0]].astype(f32)
            + travel[1, reach, order_pair[1]].astype(f32)
        )

    def order_of(way, own):
        return 1 - (0 if (way == 0) == own else 1)

    far_pair = [order_of(0, False), order_of(1, False)]
    near_pair = [order_of(0, True), order_of(1, True)]

    def trade(piece, member):
        first = pl.multiple_of(member * depth, depth)
        return begin(
            remote(
                trade_send.at[pl.ds(first, depth), :],
                trade_recv.at[piece - 1],
                trade_ss.at[piece - 1],
                trade_rs.at[piece - 1],
                peers[piece],
            )
        )

    far_rows = pl.ds(pl.multiple_of((1 - high) * half, half), half)
    near_rows = pl.ds(pl.multiple_of(high * half, half), half)
    trade_send[far_rows, :] = total_of(1 - high, far_pair).astype(bf16)
    trades = {piece: trade(piece, relative[piece]) for piece in (2, 3)}
    own_sum = total_of(high, near_pair)
    trade_send[near_rows, :] = own_sum.astype(bf16)
    trades[1] = trade(1, relative[1])
    place_of, first = slab_of(0)
    acc[place_of, pl.ds(pl.multiple_of(first + high * half, half), half), :] = own_sum

    def across(member):
        return pl.ds(pl.multiple_of(member * width, width), width)

    own_rows = pl.ds(pl.multiple_of(first + lane * depth, depth), depth)
    sum_out[:, across(lane)] = sum_ref[:, across(lane)] + acc[place_of, own_rows, :] * factor
    for piece in (1, 2, 3):
        trades[piece].wait_recv()
        there = across(relative[piece])
        sum_out[:, there] = sum_ref[:, there] + trade_recv[piece - 1].astype(f32) * factor

    for copy in sent:
        copy.wait_send()

    def drain(index):
        which, owner = lax.div(index, ring), lax.rem(index, ring)
        near_copy(which, owner).wait_send()
        far_copy(which, owner).wait_send()

    loop(0, 2 * ring, drain)


def fused_shards(
    later_input, earlier_input, cotangent, gate_weight, up_weight, down_weight, down_grad_sum
):
    ring = lax.axis_size("fs") // QUAD
    rows, model = later_input.shape
    depth, hidden = gate_weight.shape
    width, chunk, total_rows = hidden // QUAD, QUAD * depth, QUAD * rows
    reach = ring // 2
    slabs = 2 + max(2, pl.cdiv(ring, total_rows // chunk)) + 1
    dma = pltpu.SemaphoreType.DMA
    bf16, f32 = jnp.bfloat16, jnp.float32
    vmem, anywhere = pl.BlockSpec(memory_space=pltpu.VMEM), pl.BlockSpec(memory_space=pl.ANY)
    factor = (rows * lax.axis_size("fs")) ** (-0.5)
    return tuple(
        pl.pallas_call(
            functools.partial(fused_kernel, ring, factor),
            out_shape=[
                jax.ShapeDtypeStruct(later_input.shape, bf16),
                jax.ShapeDtypeStruct(earlier_input.shape, bf16),
                jax.ShapeDtypeStruct(down_grad_sum.shape, f32),
            ],
            in_specs=[anywhere] * 3 + [vmem] * 4,
            out_specs=[vmem] * 3,
            scratch_shapes=[
                pltpu.VMEM((3, model, width), bf16),
                pltpu.VMEM((3, total_rows, model), bf16),
                pltpu.VMEM((slabs, total_rows, width), f32),
                pltpu.VMEM((2, ring, 2, rows, chunk), f32),
                pltpu.VMEM((2, ring, 2, rows, chunk), bf16),
                pltpu.VMEM((2, ring, 2, rows, chunk), bf16),
                pltpu.VMEM((2, ring, rows, chunk), bf16),
                pltpu.VMEM((2, ring, rows, chunk), bf16),
                pltpu.VMEM((2, reach + 1, 2, 2 * depth, width), bf16),
                pltpu.VMEM((chunk, width), bf16),
                pltpu.VMEM((3, depth, width), bf16),
                dma((3, 3)),
                dma((3, 3)),
                dma((3, 2, QUAD)),
                dma((3, 2, QUAD)),
                dma((3, 2, reach - 1, 2)),
                dma((3, 2, reach - 1, 2)),
                dma((3, 3)),
                dma((3, 3)),
                dma((2, ring)),
                dma((2, ring)),
                dma((2, ring)),
                dma((2, ring)),
                dma((2, reach, 2)),
                dma((2, reach, 2)),
                dma((3,)),
                dma((3,)),
                dma((6,)),
            ],
            compiler_params=pltpu.CompilerParams(
                collective_id=0, has_side_effects=True, vmem_limit_bytes=67_043_328
            ),
        )(
            earlier_input,
            later_input,
            cotangent,
            gate_weight,
            up_weight,
            down_weight,
            down_grad_sum,
        )
    )


def fits(mesh):
    return mesh.shape["tp"] == 1 and mesh.shape["fs"] == 8 * QUAD


def solution(mesh):
    in_specs = (
        P(("fs", "tp"), None),
        P(("fs", "tp"), None),
        P(("fs", "tp"), None),
        P("fs", "tp"),
        P("fs", "tp"),
        P("fs", "tp"),
        P("fs", "tp"),
    )
    out_specs = (P(("fs", "tp"), None), P(("fs", "tp"), None), P("fs", "tp"))
    body = fused_shards if fits(mesh) else shards
    return jax.shard_map(body, mesh=mesh, in_specs=in_specs, out_specs=out_specs, check_vma=False)
```

time: 217 us -> 144 us (0.66)
  matrix products: 41.3 us -> 0 us
  Pallas kernels: 102 us -> 139 us
  waiting for transfers between devices: 34.4 us -> 0 us
  other arithmetic: 14.2 us -> 0 us
  between operations: 14.3 us -> 0.65 us
  starting transfers between devices: 5.66 us -> 0 us
    dot_general x8 -> x0, matrix products: 41.3 us -> none  [the longest x3 19 us: contract_last(): lax.dot_general(leading, trailing, (((1,), (1,)), ((), ())), preferred_el...]
    pallas_call x1, Pallas kernels: 102 us -> 139 us  [fused_shards(): pl.pallas_call(functools.partial(fused_kernel, ring, factor), out_shape=[...]
    ppermute x4 -> x0, waiting for transfers between devices: 15.6 us -> none  [swap(): lax.ppermute(value, 'fs', [(index, index ^ bit) for index in range(total)])]
    reduce_scatter x1 -> x0, waiting for transfers between devices: 14.3 us -> none  [quad_shards(): lax.psum_scatter(partial_sum, 'fs', scatter_dimension=0, tiled=True, axis...]
    convert_element_type x6 -> x0, other arithmetic: 11.7 us -> none  [the longest x2 5.47 us: return_tokens(): return (mine[0] + near[0] + far.astype(jnp.float32)).astype(jnp.bfloat16)]
    all_to_all x1 -> x0, waiting for transfers between devices: 4.55 us -> none  [quad_shards(): lax.all_to_all(summed, 'fs', split_axis=0, concat_axis=1, tiled=True, axi...]
    all_to_all x1 -> x0, starting transfers between devices: 3.46 us -> none  [quad_shards(): lax.all_to_all(summed, 'fs', split_axis=0, concat_axis=1, tiled=True, axi...]
    unnamed x20 -> x7, local copies, waits for them, and re-layouts: 2.67 us -> 4.46 us
  transfers between devices with their start and end apart: 6 -> 0, of which waited for: 3 -> 0; matrix products, arithmetic and copies ran while one was open for 20% -> 0% of each run, Pallas kernels for 0% -> 0%
where the time goes in v1:
time: 144 us
  Pallas kernels  139 us (97%)
  local copies, waits for them, and re-layouts  4.46 us (3%)
    pallas_call x1, Pallas kernels, fused_shards(): pl.pallas_call(functools.partial(fused_kernel, ring, factor), out_shape=[...  139 us
    unnamed x7, local copies, waits for them, and re-layouts  4.46 us

profile of v1, /device:TPU:0, one launch (start us, length us, event | category | flops | bytes accessed | tf_op | source)
XLA Modules:
  0.0 144.1 jit_solution(2925609197028515087)
XLA Ops:
  0.6 139.0 %shard_map.94 = (bf16[192,2048]{1,0:T(8,128)(2,1)}, bf16[192,2048]{1,0:T(8,128)(2,1)}, f32[64,3072]{1,0:T(8,128)}) custom-call(bf16[192,2048]{1,0:T(8,128)(2,1)} %refs_0_.1, bf16[192,2048]{1,0:T(8,128)(2,1)} %refs_1_.1, bf16[192,2048]{1,0:T(8,128)(2,1)} %refs_2_.1, bf16[64,3072]{1,0:T(8,128)(2,1)} %refs_3_.1, bf16[64,3072]{1,0:T(8,128)(2,1)} %refs_4_.1, ...), custom_call_target="tpu_custom_call" | custom-call | tf_op jit(solution)/shard_map/pallas_call | solution.py:572
  139.6 0.0 copy-start.1
  139.6 2.2 %copy.13 = bf16[192,2048]{1,0:T(8,128)(2,1)} copy(bf16[192,2048]{1,0:T(8,128)(2,1)} %get-tuple-element.6) | data formatting | bytes 1572864
  141.8 0.0 copy-done.1
  141.8 0.0 copy-start
  141.8 0.9 copy.14
  142.7 0.5 copy-done
  143.2 0.9 copy.15
Async XLA Ops:
  139.6 2.2 %copy-start.1 = (bf16[192,2048]{1,0:T(8,128)(2,1)S(1)}, bf16[192,2048]{1,0:T(8,128)(2,1)}, u32[]{:S(2)}) copy-start(bf16[192,2048]{1,0:T(8,128)(2,1)} %get-tuple-element.7) | copy-start | bytes 2359300
  141.8 1.4 copy-start

commit v2 on v1

--- a/solution.py
+++ b/solution.py
@@ -90,11 +90,13 @@
 
 
 def fused_kernel(ring, factor, *refs):
-    token_refs, weight_refs, sum_ref = refs[:3], refs[3:6], refs[6]
+    token_refs, weight_inputs, sum_input = refs[:3], refs[3:6], refs[6]
     outs, sum_out = refs[7:9], refs[9]
-    whole, tok, acc, mine, near_send, near_recv, far_send, far_recv, travel, trade_send, trade_recv = refs[10:21]
+    (staged, sum_ref, whole, tok, acc, mine, near_send, near_recv, far_send, far_recv, travel,
+     trade_send, trade_recv) = refs[10:23]
     (quad_ss, quad_rs, first_ss, first_rs, ring_ss, ring_rs, tok_ss, tok_rs, near_ss, near_rs,
-     far_ss, far_rs, sum_ss, sum_rs, trade_ss, trade_rs, local_sem) = refs[21:]
+     far_ss, far_rs, sum_ss, sum_rs, trade_ss, trade_rs, local_sem) = refs[23:]
+    weight_refs = [staged.at[weight] for weight in range(3)]
     bf16, f32 = jnp.bfloat16, jnp.float32
     me = lax.axis_index("fs")
     group, lane = lax.div(me, QUAD), lax.rem(me, QUAD)
@@ -121,6 +123,13 @@
         pl.semaphore_signal(
             barrier, inc=1, device_id={"fs": other}, device_id_type=pl.DeviceIdType.MESH
         )
+    staging = [
+        pltpu.make_async_copy(weight_inputs[weight], staged.at[weight], local_sem.at[6 + weight])
+        for weight in range(3)
+    ]
+    staging.append(pltpu.make_async_copy(sum_input, sum_ref, local_sem.at[9]))
+    for copy in staging:
+        copy.start()
     pl.semaphore_wait(barrier, QUAD + 1)
 
     def remote(source, target, send, recv, other):
@@ -152,17 +161,6 @@
         return copy
 
     quad, first_hop, hop, tokens = {}, {}, {}, {}
-    for weight in range(3):
-        for far in (1, 3, 2):
-            quad[weight, far] = begin(
-                remote(
-                    columns(weight, relative[far]),
-                    slab(weight, group, lane),
-                    quad_ss.at[weight, far - 1],
-                    quad_rs.at[weight, far - 1],
-                    peers[far],
-                )
-            )
 
     def hop_first(weight, piece):
         for way in range(2):
@@ -177,8 +175,21 @@
                 )
             )
 
-    hop_first(0, 0)
-    hop_first(1, 0)
+    for weight in range(3):
+        staging[weight].wait()
+        for far in (1, 3, 2):
+            quad[weight, far] = begin(
+                remote(
+                    columns(weight, relative[far]),
+                    slab(weight, group, lane),
+                    quad_ss.at[weight, far - 1],
+                    quad_rs.at[weight, far - 1],
+                    peers[far],
+                )
+            )
+        if weight < 2:
+            hop_first(weight, 0)
+
     for weight in range(3):
         copy = pltpu.make_async_copy(
             columns(weight, lane), slab(weight, group, lane), local_sem.at[weight]
@@ -226,7 +237,7 @@
         for piece in (3, 2):
             quad[weight, piece].wait_recv()
             hop_first(weight, piece)
-    for copy in kept:
+    for copy in kept + staging[3:]:
         copy.wait()
 
     arrived = set()
@@ -418,57 +429,32 @@
         produce(0, owner, contract_last(tok[1, :, 0:width], right))
         acc[last_slab] += jnp.dot(tok[2, :, where], right, preferred_element_type=f32)
 
-    loop(0, 3, lambda i: down_step(i - 1))
-    forward(2, 3, 1)
-    loop(0, 3, lambda i: relay(0, group_at(i - 1)))
-    loop(0, ring, partial_sum)
-
-    for step in range(3, reach + 1):
-        if step > 3:
-            for order in range(1 if step == reach else 2):
-                forward(2, step, order)
-        arrive(2, step - 1)
-        distance = step - 1
-        loop(0, 2, lambda i: down_step((2 * i - 1) * distance))
-        loop(0, 2, lambda i: relay(0, group_at((2 * i - 1) * distance)))
-
     moved = {}
 
-    def pass_on(step, order, add):
-        for way in range(2):
-            part = halves[way][1 - order]
-            shift = (reach + 1 - step) * (1 if way == 0 else -1)
-            if add:
-                moved[way, step - 1, order].wait_recv()
-                travel[way, step - 1, order] = (
-                    travel[way, step - 1, order].astype(f32) + own_part(shift, part)
-                ).astype(bf16)
-            else:
-                travel[way, step - 1, order] = own_part(shift, part).astype(bf16)
-        for way in range(2):
-            moved[way, step, order] = begin(
-                remote(
-                    travel.at[way, step - 1, order],
-                    travel.at[way, step, order],
-                    sum_ss.at[way, step - 1, order],
-                    sum_rs.at[way, step - 1, order],
-                    around[way],
-                )
+    def pass_on(way, step, order, add=True):
+        part = halves[way][order]
+        shift = (reach + 1 - step) * (1 if way == 0 else -1)
+        slot = travel.at[way, step - 1, order]
+        if add:
+            moved[way, step - 1, order].wait_recv()
+            slot[...] = (slot[...].astype(f32) + own_part(shift, part)).astype(bf16)
+        else:
+            slot[...] = own_part(shift, part).astype(bf16)
+        moved[way, step, order] = begin(
+            remote(
+                slot,
+                travel.at[way, step, order],
+                sum_ss.at[way, step - 1, order],
+                sum_rs.at[way, step - 1, order],
+                around[way],
             )
-
-    pass_on(1, 1, False)
-    pass_on(2, 0, False)
-    arrive(2, reach)
-    down_step(reach)
+        )
 
     def grads(index):
         where = pl.ds(pl.multiple_of(index * tile, tile), tile)
         hidden = acc[last_slab, where, :]
         tok[0, where, width : 2 * width] = (hidden * acc[0, where, :]).astype(bf16)
         tok[1, where, width : 2 * width] = (hidden * acc[1, where, :]).astype(bf16)
-
-    loop(0, total_rows // tile, grads)
-    relay(0, group_at(reach))
 
     def input_step(owner):
         where = span(owner)
@@ -483,19 +469,47 @@
         def _():
             relay(1, owner - 1)
 
-    pauses = [(2, 1)] + [(step, order) for step in range(3, reach + 1) for order in (0, 1)]
-    stops = [ring // 4, ring // 2 + 1, ring]
-    first = 0
-    for stop in stops:
-        loop(first, stop, input_step)
-        first = stop
-        if pauses:
-            pass_on(*pauses.pop(0), True)
+    def both(distance, body):
+        loop(0, 2, lambda i: body((2 * i - 1) * distance))
+
+    def relay_at(shift):
+        relay(0, group_at(shift))
+
+    loop(0, 3, lambda i: down_step(i - 1))
+    forward(2, 3, 1)
+    loop(0, 3, lambda i: relay_at(i - 1))
+    loop(reach - 1, reach + 2, partial_sum)
+    pass_on(0, 1, 1, False)
+    forward(2, reach, 0)
+    pass_on(1, 1, 1, False)
+    pass_on(1, 2, 0, False)
+    loop(0, ring - 3, lambda i: partial_sum(lax.rem(reach + 2 + i, ring)))
+    for distance in range(2, reach):
+        arrive(2, distance)
+        both(distance, down_step)
+        both(distance, relay_at)
+    pass_on(0, 2, 1)
+    pass_on(0, 2, 0, False)
+    arrive(2, reach)
+    pass_on(1, 2, 1)
+    down_step(reach)
+    loop(0, total_rows // tile, grads)
+    relay_at(reach)
+    loop(0, ring // 2 - 1, input_step)
+    pass_on(0, 3, 1)
+    pass_on(1, 3, 0)
+    loop(ring // 2 - 1, ring - 1, input_step)
+    pass_on(0, 3, 0)
+    pass_on(1, 3, 1)
+    loop(ring - 1, ring, input_step)
     relay(1, ring - 1)
     loop(0, ring, lambda i: finish(0, i))
-    while pauses:
-        pass_on(*pauses.pop(0), True)
-    loop(0, ring, lambda i: finish(1, i))
+    pass_on(0, 4, 1)
+    pass_on(1, 4, 0)
+    loop(0, ring // 2, lambda i: finish(1, i))
+    pass_on(0, 4, 0)
+    pass_on(1, 4, 1)
+    loop(ring // 2, ring - 2, lambda i: finish(1, i))
 
     def total_of(part, order_pair):
         for way in range(2):
@@ -506,11 +520,7 @@
             + travel[1, reach, order_pair[1]].astype(f32)
         )
 
-    def order_of(way, own):
-        return 1 - (0 if (way == 0) == own else 1)
-
-    far_pair = [order_of(0, False), order_of(1, False)]
-    near_pair = [order_of(0, True), order_of(1, True)]
+    far_pair, near_pair = (1, 0), (0, 1)
 
     def trade(piece, member):
         first = pl.multiple_of(member * depth, depth)
@@ -528,6 +538,7 @@
     near_rows = pl.ds(pl.multiple_of(high * half, half), half)
     trade_send[far_rows, :] = total_of(1 - high, far_pair).astype(bf16)
     trades = {piece: trade(piece, relative[piece]) for piece in (2, 3)}
+    loop(ring - 2, ring, lambda i: finish(1, i))
     own_sum = total_of(high, near_pair)
     trade_send[near_rows, :] = own_sum.astype(bf16)
     trades[1] = trade(1, relative[1])
@@ -572,13 +583,15 @@
         pl.pallas_call(
             functools.partial(fused_kernel, ring, factor),
             out_shape=[
-                jax.ShapeDtypeStruct(later_input.shape, bf16),
-                jax.ShapeDtypeStruct(earlier_input.shape, bf16),
-                jax.ShapeDtypeStruct(down_grad_sum.shape, f32),
+                pltpu.VMEM(later_input.shape, bf16),
+                pltpu.VMEM(earlier_input.shape, bf16),
+                pltpu.VMEM(down_grad_sum.shape, f32),
             ],
-            in_specs=[anywhere] * 3 + [vmem] * 4,
+            in_specs=[anywhere] * 7,
             out_specs=[vmem] * 3,
             scratch_shapes=[
+                pltpu.VMEM((3, depth, hidden), bf16),
+                pltpu.VMEM((depth, hidden), f32),
                 pltpu.VMEM((3, model, width), bf16),
                 pltpu.VMEM((3, total_rows, model), bf16),
                 pltpu.VMEM((slabs, total_rows, width), f32),
@@ -606,10 +619,10 @@
                 dma((2, reach, 2)),
                 dma((3,)),
                 dma((3,)),
-                dma((6,)),
+                dma((10,)),
             ],
             compiler_params=pltpu.CompilerParams(
-                collective_id=0, has_side_effects=True, vmem_limit_bytes=67_043_328
+                collective_id=0, has_side_effects=True, vmem_limit_bytes=62_000_000
             ),
         )(
             earlier_input,

time: 144 us -> 132 us (0.917)
  Pallas kernels: 139 us -> 128 us
  local copies, waits for them, and re-layouts: 4.46 us -> 2.64 us
    pallas_call x1, Pallas kernels: 139 us -> 128 us  [fused_shards(): pl.pallas_call(functools.partial(fused_kernel, ring, factor), out_shape=[...]
    unnamed x7 -> x3, local copies, waits for them, and re-layouts: 4.46 us -> 2.64 us
where the time goes in v2:
time: 132 us
  Pallas kernels  128 us (97%)
  local copies, waits for them, and re-layouts  2.64 us (2%)
    pallas_call x1, Pallas kernels, fused_shards(): pl.pallas_call(functools.partial(fused_kernel, ring, factor), out_shape=[...  128 us
    unnamed x3, local copies, waits for them, and re-layouts  2.64 us

profile of v2, /device:TPU:0, one launch (start us, length us, event | category | flops | bytes accessed | tf_op | source)
XLA Modules:
  0.0 131.7 jit_solution(12229680479550052502)
XLA Ops:
  0.6 128.4 %shard_map.94 = (bf16[192,2048]{1,0:T(8,128)(2,1)S(1)}, bf16[192,2048]{1,0:T(8,128)(2,1)S(1)}, f32[64,3072]{1,0:T(8,128)S(1)}) custom-call(bf16[192,2048]{1,0:T(8,128)(2,1)} %refs_0_.1, bf16[192,2048]{1,0:T(8,128)(2,1)} %refs_1_.1, bf16[192,2048]{1,0:T(8,128)(2,1)} %refs_2_.1, bf16[64,3072]{1,0:T(8,128)(2,1)} %refs_3_.1, bf16[64,3072]{1,0:T(8,128)(2,1)} %refs_4_.1, ...), custom_call_target="tpu_custom_call" | custom-call | tf_op jit(solution)/shard_map/pallas_call | solution.py:583
  129.0 0.9 copy.13
  129.9 0.9 copy.14
  130.8 0.9 copy.15

commit v3 on v2

--- a/solution.py
+++ b/solution.py
@@ -94,8 +94,8 @@
     outs, sum_out = refs[7:9], refs[9]
     (staged, sum_ref, whole, tok, acc, mine, near_send, near_recv, far_send, far_recv, travel,
      trade_send, trade_recv) = refs[10:23]
-    (quad_ss, quad_rs, first_ss, first_rs, ring_ss, ring_rs, tok_ss, tok_rs, near_ss, near_rs,
-     far_ss, far_rs, sum_ss, sum_rs, trade_ss, trade_rs, local_sem) = refs[23:]
+    (quad_ss, quad_rs, first_rs, ring_ss, ring_rs, tok_ss, tok_rs, near_ss, near_rs,
+     far_ss, far_rs, sum_ss, sum_rs, last_rs, trade_ss, trade_rs, local_sem) = refs[23:]
     weight_refs = [staged.at[weight] for weight in range(3)]
     bf16, f32 = jnp.bfloat16, jnp.float32
     me = lax.axis_index("fs")
@@ -124,10 +124,10 @@
             barrier, inc=1, device_id={"fs": other}, device_id_type=pl.DeviceIdType.MESH
         )
     staging = [
-        pltpu.make_async_copy(weight_inputs[weight], staged.at[weight], local_sem.at[6 + weight])
+        pltpu.make_async_copy(weight_inputs[weight], staged.at[weight], local_sem.at[2 + weight])
         for weight in range(3)
     ]
-    staging.append(pltpu.make_async_copy(sum_input, sum_ref, local_sem.at[9]))
+    staging.append(pltpu.make_async_copy(sum_input, sum_ref, local_sem.at[5]))
     for copy in staging:
         copy.start()
     pl.semaphore_wait(barrier, QUAD + 1)
@@ -153,12 +153,12 @@
         first = pl.multiple_of(owner * chunk + part * half, half)
         return whole.at[weight, pl.ds(first, half), :]
 
-    sent, kept = [], []
-
     def begin(copy):
         copy.start()
-        sent.append(copy)
         return copy
+
+    def settle(part, send):
+        remote(part, part, send, send, peers[1]).wait_send()
 
     quad, first_hop, hop, tokens = {}, {}, {}, {}
 
@@ -169,8 +169,8 @@
                 remote(
                     columns(weight, lane) if piece == 0 else target,
                     target,
-                    first_ss.at[weight, way, piece],
-                    first_rs.at[weight, way, piece],
+                    ring_ss.at[weight, way],
+                    first_rs.at[weight, way, 0 if piece < 2 else 1],
                     around[way],
                 )
             )
@@ -182,7 +182,7 @@
                 remote(
                     columns(weight, relative[far]),
                     slab(weight, group, lane),
-                    quad_ss.at[weight, far - 1],
+                    quad_ss.at[weight],
                     quad_rs.at[weight, far - 1],
                     peers[far],
                 )
@@ -192,10 +192,9 @@
 
     for weight in range(3):
         copy = pltpu.make_async_copy(
-            columns(weight, lane), slab(weight, group, lane), local_sem.at[weight]
+            columns(weight, lane), slab(weight, group, lane), local_sem.at[0]
         )
         copy.start()
-        kept.append(copy)
 
     def row_block(token, block):
         return tok.at[token, pl.ds(block * rows, rows), :]
@@ -205,7 +204,7 @@
             remote(
                 source,
                 row_block(token, block),
-                tok_ss.at[token, slot],
+                tok_ss.at[token],
                 tok_rs.at[token, slot],
                 other,
             )
@@ -215,10 +214,9 @@
         send_rows(token, token_refs[token], 2, 1, peers[2])
         send_rows(token, token_refs[token], 1, 0, peers[1])
         copy = pltpu.make_async_copy(
-            token_refs[token], row_block(token, 0), local_sem.at[3 + token]
+            token_refs[token], row_block(token, 0), local_sem.at[1]
         )
         copy.start()
-        kept.append(copy)
 
     def clear(index, carry):
         acc[index] = jnp.zeros(acc.shape[1:], f32)
@@ -237,8 +235,9 @@
         for piece in (3, 2):
             quad[weight, piece].wait_recv()
             hop_first(weight, piece)
-    for copy in kept + staging[3:]:
-        copy.wait()
+    staging[3].wait()
+    for part, index in ((whole.at[0, 0 : 3 * depth], 0), (tok.at[0, 0 : 3 * rows], 1)):
+        pltpu.make_async_copy(part, part, local_sem.at[index]).wait()
 
     arrived = set()
 
@@ -247,9 +246,10 @@
             return
         arrived.add((weight, way, step, order))
         if step == 1:
-            own_half = (order == 0) == (way == 0)
-            for piece in (0, 1) if own_half else (3, 2):
-                first_hop[weight, way, piece].wait_recv()
+            side = 0 if (order == 0) == (way == 0) else 1
+            part = half_slab(weight, group_at(-1 if way == 0 else 1), halves[way][order])
+            slot = first_rs.at[weight, way, side]
+            remote(part, part, slot, slot, peers[1]).wait_recv()
         else:
             hop[weight, way, step, order].wait_recv()
 
@@ -262,7 +262,7 @@
                 remote(
                     part,
                     part,
-                    ring_ss.at[weight, way, step - 2, order],
+                    ring_ss.at[weight, way],
                     ring_rs.at[weight, way, step - 2, order],
                     around[way],
                 )
@@ -339,9 +339,7 @@
         arrive(weight, reach)
     project_pair(reach, [0, 1])
     for token in range(2):
-        for slot in range(3):
-            tokens[token, slot].wait_send()
-            sent[:] = [copy for copy in sent if copy is not tokens[token, slot]]
+        settle(tok.at[token, 0 : 3 * rows], tok_ss.at[token])
 
     tile = 32
 
@@ -385,7 +383,7 @@
         return remote(
             near_send.at[which, owner],
             near_recv.at[which, owner],
-            near_ss.at[which, owner],
+            near_ss.at[which],
             near_rs.at[which, owner],
             peers[1],
         )
@@ -394,7 +392,7 @@
         return remote(
             far_send.at[which, owner],
             far_recv.at[which, owner],
-            far_ss.at[which, owner],
+            far_ss.at[which],
             far_rs.at[which, owner],
             peers[2],
         )
@@ -440,11 +438,24 @@
             slot[...] = (slot[...].astype(f32) + own_part(shift, part)).astype(bf16)
         else:
             slot[...] = own_part(shift, part).astype(bf16)
+        if step == reach and order == way:
+            for index, member in enumerate((1 - low, low)):
+                where = pl.ds(pl.multiple_of(member * depth, depth), depth)
+                moved[way, step, order, index] = begin(
+                    remote(
+                        slot.at[where, :],
+                        travel.at[way, step, order, where, :],
+                        sum_ss.at[way],
+                        last_rs.at[way, index],
+                        around[way],
+                    )
+                )
+            return
         moved[way, step, order] = begin(
             remote(
                 slot,
                 travel.at[way, step, order],
-                sum_ss.at[way, step - 1, order],
+                sum_ss.at[way],
                 sum_rs.at[way, step - 1, order],
                 around[way],
             )
@@ -511,59 +522,76 @@
     pass_on(1, 4, 1)
     loop(ring // 2, ring - 2, lambda i: finish(1, i))
 
-    def total_of(part, order_pair):
-        for way in range(2):
-            moved[way, reach, order_pair[way]].wait_recv()
-        return (
-            own_part(0, part)
-            + travel[0, reach, order_pair[0]].astype(f32)
-            + travel[1, reach, order_pair[1]].astype(f32)
-        )
-
-    far_pair, near_pair = (1, 0), (0, 1)
-
     def trade(piece, member):
         first = pl.multiple_of(member * depth, depth)
         return begin(
             remote(
                 trade_send.at[pl.ds(first, depth), :],
                 trade_recv.at[piece - 1],
-                trade_ss.at[piece - 1],
+                trade_ss.at[0],
                 trade_rs.at[piece - 1],
                 peers[piece],
             )
         )
 
-    far_rows = pl.ds(pl.multiple_of((1 - high) * half, half), half)
-    near_rows = pl.ds(pl.multiple_of(high * half, half), half)
-    trade_send[far_rows, :] = total_of(1 - high, far_pair).astype(bf16)
-    trades = {piece: trade(piece, relative[piece]) for piece in (2, 3)}
-    loop(ring - 2, ring, lambda i: finish(1, i))
-    own_sum = total_of(high, near_pair)
-    trade_send[near_rows, :] = own_sum.astype(bf16)
-    trades[1] = trade(1, relative[1])
-    place_of, first = slab_of(0)
-    acc[place_of, pl.ds(pl.multiple_of(first + high * half, half), half), :] = own_sum
-
     def across(member):
         return pl.ds(pl.multiple_of(member * width, width), width)
 
-    own_rows = pl.ds(pl.multiple_of(first + lane * depth, depth), depth)
-    sum_out[:, across(lane)] = sum_ref[:, across(lane)] + acc[place_of, own_rows, :] * factor
-    for piece in (1, 2, 3):
+    def collect(piece):
         trades[piece].wait_recv()
         there = across(relative[piece])
         sum_out[:, there] = sum_ref[:, there] + trade_recv[piece - 1].astype(f32) * factor
 
-    for copy in sent:
-        copy.wait_send()
-
-    def drain(index):
-        which, owner = lax.div(index, ring), lax.rem(index, ring)
-        near_copy(which, owner).wait_send()
-        far_copy(which, owner).wait_send()
-
-    loop(0, 2 * ring, drain)
+    def near_total(index, member):
+        where = pl.ds(pl.multiple_of(member * depth, depth), depth)
+        for way in range(2):
+            moved[way, reach, way, index].wait_recv()
+        rows_of = pl.ds(pl.multiple_of(first + high * half + member * depth, depth), depth)
+        return (
+            acc[place_of, rows_of, :]
+            + travel[0, reach, 0, where, :].astype(f32)
+            + travel[1, reach, 1, where, :].astype(f32)
+        )
+
+    place_of, first = slab_of(0)
+    moved[0, reach, 1].wait_recv()
+    moved[1, reach, 0].wait_recv()
+    trade_send[pl.ds(pl.multiple_of((1 - high) * half, half), half), :] = (
+        own_part(0, 1 - high) + travel[0, reach, 1].astype(f32) + travel[1, reach, 0].astype(f32)
+    ).astype(bf16)
+    trades = {piece: trade(piece, relative[piece]) for piece in (2, 3)}
+    loop(ring - 2, ring, lambda i: finish(1, i))
+    trade_send[pl.ds(pl.multiple_of(relative[1] * depth, depth), depth), :] = near_total(
+        0, 1 - low
+    ).astype(bf16)
+    trades[1] = trade(1, relative[1])
+    collect(2)
+    collect(3)
+    sum_out[:, across(lane)] = sum_ref[:, across(lane)] + near_total(1, low) * factor
+    collect(1)
+
+    for weight in range(3):
+        settle(whole.at[weight, 0 : 3 * depth], quad_ss.at[weight])
+        for way in range(2):
+            settle(whole.at[weight, 0 : (2 * reach - 1) * half], ring_ss.at[weight, way])
+    settle(tok.at[2, 0 : 3 * rows], tok_ss.at[2])
+    for index in range(2):
+        settle(near_send.at[index], near_ss.at[index])
+        settle(far_send.at[index], far_ss.at[index])
+        settle(whole.at[0, 0 : (2 * reach - 1) * half], sum_ss.at[index])
+    settle(trade_recv, trade_ss.at[0])
+
+
+def deliver_kernel(*refs):
+    sources, targets, done = refs[:3], refs[3:6], refs[6]
+    copies = [
+        pltpu.make_async_copy(source, target, done.at[index])
+        for index, (source, target) in enumerate(zip(sources, targets))
+    ]
+    for copy in copies:
+        copy.start()
+    for copy in copies:
+        copy.wait()
 
 
 def fused_shards(
@@ -579,14 +607,14 @@
     bf16, f32 = jnp.bfloat16, jnp.float32
     vmem, anywhere = pl.BlockSpec(memory_space=pltpu.VMEM), pl.BlockSpec(memory_space=pl.ANY)
     factor = (rows * lax.axis_size("fs")) ** (-0.5)
-    return tuple(
-        pl.pallas_call(
+    shapes = [
+        (later_input.shape, bf16),
+        (earlier_input.shape, bf16),
+        (down_grad_sum.shape, f32),
+    ]
+    results = pl.pallas_call(
             functools.partial(fused_kernel, ring, factor),
-            out_shape=[
-                pltpu.VMEM(later_input.shape, bf16),
-                pltpu.VMEM(earlier_input.shape, bf16),
-                pltpu.VMEM(down_grad_sum.shape, f32),
-            ],
+            out_shape=[pltpu.VMEM(*shape) for shape in shapes],
             in_specs=[anywhere] * 7,
             out_specs=[vmem] * 3,
             scratch_shapes=[
@@ -603,23 +631,23 @@
                 pltpu.VMEM((2, reach + 1, 2, 2 * depth, width), bf16),
                 pltpu.VMEM((chunk, width), bf16),
                 pltpu.VMEM((3, depth, width), bf16),
+                dma((3,)),
                 dma((3, 3)),
+                dma((3, 2, 2)),
+                dma((3, 2)),
+                dma((3, 2, reach - 1, 2)),
+                dma((3,)),
                 dma((3, 3)),
-                dma((3, 2, QUAD)),
-                dma((3, 2, QUAD)),
-                dma((3, 2, reach - 1, 2)),
-                dma((3, 2, reach - 1, 2)),
-                dma((3, 3)),
-                dma((3, 3)),
+                dma((2,)),
                 dma((2, ring)),
+                dma((2,)),
                 dma((2, ring)),
-                dma((2, ring)),
-                dma((2, ring)),
+                dma((2,)),
                 dma((2, reach, 2)),
-                dma((2, reach, 2)),
+                dma((2, 2)),
+                dma((1,)),
                 dma((3,)),
-                dma((3,)),
-                dma((10,)),
+                dma((6,)),
             ],
             compiler_params=pltpu.CompilerParams(
                 collective_id=0, has_side_effects=True, vmem_limit_bytes=62_000_000
@@ -633,6 +661,15 @@
             down_weight,
             down_grad_sum,
         )
+    return tuple(
+        pl.pallas_call(
+            deliver_kernel,
+            out_shape=[jax.ShapeDtypeStruct(*shape) for shape in shapes],
+            in_specs=[vmem] * 3,
+            out_specs=[anywhere] * 3,
+            scratch_shapes=[dma((3,))],
+            compiler_params=pltpu.CompilerParams(vmem_limit_bytes=1_000_000),
+        )(*(pltpu.with_memory_space_constraint(value, pltpu.VMEM) for value in results))
     )
 
 

time: 132 us -> 130 us (0.985)
  local copies, waits for them, and re-layouts: 2.64 us -> 0 us
    unnamed x3 -> x0, local copies, waits for them, and re-layouts: 2.64 us -> none
    pallas_call x0 -> x1, Pallas kernels: none -> 1.43 us  [fused_shards(): pl.pallas_call(deliver_kernel, out_shape=[jax.ShapeDtypeStruct(*shape) fo...]
where the time goes in v3:
time: 130 us; the launch traced here: 129 us
  Pallas kernels  129 us (99%)
    pallas_call x1, Pallas kernels, fused_shards(): pl.pallas_call(functools.partial(fused_kernel, ring, factor), out_shape=[...  127 us

profile of v3, /device:TPU:0, one launch (start us, length us, event | category | flops | bytes accessed | tf_op | source)
XLA Modules:
  0.0 129.2 jit_solution(13932544276022542187)
XLA Ops:
  0.6 127.2 %shard_map.94 = (bf16[192,2048]{1,0:T(8,128)(2,1)S(1)}, bf16[192,2048]{1,0:T(8,128)(2,1)S(1)}, f32[64,3072]{1,0:T(8,128)S(1)}) custom-call(bf16[192,2048]{1,0:T(8,128)(2,1)} %refs_0_.1, bf16[192,2048]{1,0:T(8,128)(2,1)} %refs_1_.1, bf16[192,2048]{1,0:T(8,128)(2,1)} %refs_2_.1, bf16[64,3072]{1,0:T(8,128)(2,1)} %refs_3_.1, bf16[64,3072]{1,0:T(8,128)(2,1)} %refs_4_.1, ...), custom_call_target="tpu_custom_call" | custom-call | tf_op jit(solution)/shard_map/pallas_call | solution.py:615
  127.8 1.4 %shard_map.95 = (bf16[192,2048]{1,0:T(8,128)(2,1)}, bf16[192,2048]{1,0:T(8,128)(2,1)}, f32[64,3072]{1,0:T(8,128)}) custom-call(bf16[192,2048]{1,0:T(8,128)(2,1)S(1)} %get-tuple-element.6.refs_0_, bf16[192,2048]{1,0:T(8,128)(2,1)S(1)} %get-tuple-element.7.refs_1_, f32[64,3072]{1,0:T(8,128)S(1)} %get-tuple-element.8.refs_2_), custom_call_target="tpu_custom_call" | custom-call | tf_op jit(solution)/shard_map/pallas_call | solution.py:665

commit v4 on v3

--- a/solution.py
+++ b/solution.py
@@ -95,7 +95,7 @@
     (staged, sum_ref, whole, tok, acc, mine, near_send, near_recv, far_send, far_recv, travel,
      trade_send, trade_recv) = refs[10:23]
     (quad_ss, quad_rs, first_rs, ring_ss, ring_rs, tok_ss, tok_rs, near_ss, near_rs,
-     far_ss, far_rs, sum_ss, sum_rs, last_rs, trade_ss, trade_rs, local_sem) = refs[23:]
+     far_ss, far_rs, sum_ss, sum_rs, trade_ss, trade_rs, local_sem) = refs[23:]
     weight_refs = [staged.at[weight] for weight in range(3)]
     bf16, f32 = jnp.bfloat16, jnp.float32
     me = lax.axis_index("fs")
@@ -357,10 +357,7 @@
         gate, up = acc[2, where, :], acc[3, where, :]
         tok[1, where, 0:width] = (gate * jax.nn.sigmoid(gate) * up).astype(bf16)
 
-    loop(0, total_rows // tile, early_values)
-    forward(2, 3, 0)
     loop(0, total_rows // tile, later_values)
-    token_in(2)
 
     def slab_of(index):
         if isinstance(index, int):
@@ -420,46 +417,55 @@
 
     last_slab = acc.shape[0] - 1
 
-    def down_step(shift):
+    def output_step(shift):
         owner = group_at(shift)
-        where = span(owner)
-        right = whole[2, where, :]
-        produce(0, owner, contract_last(tok[1, :, 0:width], right))
-        acc[last_slab] += jnp.dot(tok[2, :, where], right, preferred_element_type=f32)
+        produce(0, owner, contract_last(tok[1, :, 0:width], whole[2, span(owner), :]))
+
+    def hidden_step(shift):
+        where = span(group_at(shift))
+        acc[last_slab] += jnp.dot(
+            tok[2, :, where], whole[2, where, :], preferred_element_type=f32
+        )
 
     moved = {}
 
-    def pass_on(way, step, order, add=True):
+    def piece_rows(piece):
+        return pl.ds(pl.multiple_of((low if piece else 1 - low) * depth, depth), depth)
+
+    def fold(way, step, order, add=True, piece=None):
         part = halves[way][order]
         shift = (reach + 1 - step) * (1 if way == 0 else -1)
-        slot = travel.at[way, step - 1, order]
+        where = slice(None) if piece is None else piece_rows(piece)
+        slot = travel.at[way, step - 1, order, where, :]
+        if piece is None:
+            mine_part = own_part(shift, part)
+        else:
+            place_of, first = slab_of((shift + ring) % ring)
+            member = low if piece else 1 - low
+            first = pl.multiple_of(first + part * half + member * depth, depth)
+            mine_part = acc[place_of, pl.ds(first, depth), :]
         if add:
-            moved[way, step - 1, order].wait_recv()
-            slot[...] = (slot[...].astype(f32) + own_part(shift, part)).astype(bf16)
+            copies = moved[way, step - 1, order]
+            for copy in copies if piece is None else copies[piece : piece + 1]:
+                copy.wait_recv()
+            slot[...] = (slot[...].astype(f32) + mine_part).astype(bf16)
         else:
-            slot[...] = own_part(shift, part).astype(bf16)
-        if step == reach and order == way:
-            for index, member in enumerate((1 - low, low)):
-                where = pl.ds(pl.multiple_of(member * depth, depth), depth)
-                moved[way, step, order, index] = begin(
+            slot[...] = mine_part.astype(bf16)
+
+    def pass_on(way, step, order, pieces=(None,)):
+        for piece in pieces:
+            where = slice(None) if piece is None else piece_rows(piece)
+            moved.setdefault((way, step, order), []).append(
+                begin(
                     remote(
-                        slot.at[where, :],
+                        travel.at[way, step - 1, order, where, :],
                         travel.at[way, step, order, where, :],
                         sum_ss.at[way],
-                        last_rs.at[way, index],
+                        sum_rs.at[way, step - 1, order, piece or 0],
                         around[way],
                     )
                 )
-            return
-        moved[way, step, order] = begin(
-            remote(
-                slot,
-                travel.at[way, step, order],
-                sum_ss.at[way],
-                sum_rs.at[way, step - 1, order],
-                around[way],
             )
-        )
 
     def grads(index):
         where = pl.ds(pl.multiple_of(index * tile, tile), tile)
@@ -486,41 +492,78 @@
     def relay_at(shift):
         relay(0, group_at(shift))
 
-    loop(0, 3, lambda i: down_step(i - 1))
+    def output_near(index):
+        output_step(index - 1)
+
+        @pl.when(index > 0)
+        def _():
+            relay_at(index - 2)
+
+    def output_pair(distance):
+        both(distance, output_step)
+        both(distance, relay_at)
+
+    loop(0, 3, output_near)
+    forward(2, 3, 0)
+    loop(0, total_rows // tile, early_values)
+    relay_at(1)
+    token_in(2)
+    loop(reach - 1, reach + 2, partial_sum)
+    loop(0, 2, lambda i: hidden_step(i - 1))
     forward(2, 3, 1)
-    loop(0, 3, lambda i: relay_at(i - 1))
-    loop(reach - 1, reach + 2, partial_sum)
-    pass_on(0, 1, 1, False)
+    arrive(2, 2)
+    output_pair(2)
     forward(2, reach, 0)
-    pass_on(1, 1, 1, False)
-    pass_on(1, 2, 0, False)
+    for way in range(2):
+        fold(way, 1, 1, False)
+        pass_on(way, 1, 1, (None,) if way else (0, 1))
+        fold(way, 2, 0, False)
+        pass_on(way, 2, 0, (None,) if way else (0,))
+
+    def step_piece(step, order, piece):
+        fold(0, step, order, True, piece)
+        pass_on(0, step, order, (piece,))
+
+    hidden_step(1)
+    both(2, hidden_step)
     loop(0, ring - 3, lambda i: partial_sum(lax.rem(reach + 2 + i, ring)))
-    for distance in range(2, reach):
-        arrive(2, distance)
-        both(distance, down_step)
-        both(distance, relay_at)
-    pass_on(0, 2, 1)
-    pass_on(0, 2, 0, False)
+    arrive(2, reach - 1)
+    output_pair(reach - 1)
+    both(reach - 1, hidden_step)
     arrive(2, reach)
+    output_step(reach)
+    hidden_step(reach)
+    loop(0, total_rows // tile, grads)
+    step_piece(2, 1, 0)
+    relay_at(reach)
+    loop(0, ring // 4, input_step)
+    step_piece(2, 1, 1)
+    pass_on(0, 2, 0, (1,))
+    fold(1, 2, 1)
     pass_on(1, 2, 1)
-    down_step(reach)
-    loop(0, total_rows // tile, grads)
-    relay_at(reach)
-    loop(0, ring // 2 - 1, input_step)
-    pass_on(0, 3, 1)
+    loop(ring // 4, ring - 2, input_step)
+    step_piece(3, 1, 0)
+    fold(1, 3, 0)
     pass_on(1, 3, 0)
-    loop(ring // 2 - 1, ring - 1, input_step)
-    pass_on(0, 3, 0)
-    pass_on(1, 3, 1)
-    loop(ring - 1, ring, input_step)
+    loop(ring - 2, ring, input_step)
+    step_piece(3, 1, 1)
+    step_piece(3, 0, 0)
     relay(1, ring - 1)
     loop(0, ring, lambda i: finish(0, i))
-    pass_on(0, 4, 1)
-    pass_on(1, 4, 0)
+    step_piece(3, 0, 1)
+    fold(1, 3, 1)
+    pass_on(1, 3, 1)
     loop(0, ring // 2, lambda i: finish(1, i))
-    pass_on(0, 4, 0)
-    pass_on(1, 4, 1)
-    loop(ring // 2, ring - 2, lambda i: finish(1, i))
+    step_piece(4, 1, 0)
+    step_piece(4, 1, 1)
+    fold(1, 4, 0)
+    pass_on(1, 4, 0, (0, 1))
+    loop(ring // 2, ring // 2 + 1, lambda i: finish(1, i))
+    step_piece(4, 0, 0)
+    step_piece(4, 0, 1)
+    fold(1, 4, 1)
+    pass_on(1, 4, 1, (0, 1))
+    loop(ring // 2 + 1, ring - 1, lambda i: finish(1, i))
 
     def trade(piece, member):
         first = pl.multiple_of(member * depth, depth)
@@ -542,32 +585,32 @@
         there = across(relative[piece])
         sum_out[:, there] = sum_ref[:, there] + trade_recv[piece - 1].astype(f32) * factor
 
-    def near_total(index, member):
-        where = pl.ds(pl.multiple_of(member * depth, depth), depth)
+    place_of, first = slab_of(0)
+
+    def total(part, orders, piece):
+        where = piece_rows(piece)
+        member = low if piece else 1 - low
+        mine_rows = pl.ds(pl.multiple_of(first + part * half + member * depth, depth), depth)
+        result = acc[place_of, mine_rows, :]
         for way in range(2):
-            moved[way, reach, way, index].wait_recv()
-        rows_of = pl.ds(pl.multiple_of(first + high * half + member * depth, depth), depth)
-        return (
-            acc[place_of, rows_of, :]
-            + travel[0, reach, 0, where, :].astype(f32)
-            + travel[1, reach, 1, where, :].astype(f32)
-        )
-
-    place_of, first = slab_of(0)
-    moved[0, reach, 1].wait_recv()
-    moved[1, reach, 0].wait_recv()
-    trade_send[pl.ds(pl.multiple_of((1 - high) * half, half), half), :] = (
-        own_part(0, 1 - high) + travel[0, reach, 1].astype(f32) + travel[1, reach, 0].astype(f32)
-    ).astype(bf16)
-    trades = {piece: trade(piece, relative[piece]) for piece in (2, 3)}
-    loop(ring - 2, ring, lambda i: finish(1, i))
-    trade_send[pl.ds(pl.multiple_of(relative[1] * depth, depth), depth), :] = near_total(
-        0, 1 - low
-    ).astype(bf16)
-    trades[1] = trade(1, relative[1])
+            moved[way, reach, orders[way]][piece].wait_recv()
+            result = result + travel[way, reach, orders[way], where, :].astype(f32)
+        return result
+
+    trades = {}
+
+    def give(piece, part, orders, index):
+        first_row = pl.multiple_of(relative[piece] * depth, depth)
+        trade_send[pl.ds(first_row, depth), :] = total(part, orders, index).astype(bf16)
+        trades[piece] = trade(piece, relative[piece])
+
+    give(3, 1 - high, (1, 0), 0)
+    loop(ring - 1, ring, lambda i: finish(1, i))
+    give(2, 1 - high, (1, 0), 1)
+    give(1, high, (0, 1), 0)
+    collect(3)
+    sum_out[:, across(lane)] = sum_ref[:, across(lane)] + total(high, (0, 1), 1) * factor
     collect(2)
-    collect(3)
-    sum_out[:, across(lane)] = sum_ref[:, across(lane)] + near_total(1, low) * factor
     collect(1)
 
     for weight in range(3):
@@ -643,8 +686,7 @@
                 dma((2,)),
                 dma((2, ring)),
                 dma((2,)),
-                dma((2, reach, 2)),
-                dma((2, 2)),
+                dma((2, reach, 2, 2)),
                 dma((1,)),
                 dma((3,)),
                 dma((6,)),

time: 130 us -> 127 us (0.977)
  Pallas kernels: 129 us -> 126 us
    pallas_call x1, Pallas kernels: 127 us -> 125 us  [fused_shards(): pl.pallas_call(functools.partial(fused_kernel, ring, factor), out_shape=[...]
where the time goes in v4:
time: 127 us
  Pallas kernels  126 us (99%)
    pallas_call x1, Pallas kernels, fused_shards(): pl.pallas_call(functools.partial(fused_kernel, ring, factor), out_shape=[...  125 us

profile of v4, /device:TPU:0, one launch (start us, length us, event | category | flops | bytes accessed | tf_op | source)
XLA Modules:
  0.0 127.1 jit_solution(2906772697947711069)
XLA Ops:
  0.6 125.0 %shard_map.94 = (bf16[192,2048]{1,0:T(8,128)(2,1)S(1)}, bf16[192,2048]{1,0:T(8,128)(2,1)S(1)}, f32[64,3072]{1,0:T(8,128)S(1)}) custom-call(bf16[192,2048]{1,0:T(8,128)(2,1)} %refs_0_.1, bf16[192,2048]{1,0:T(8,128)(2,1)} %refs_1_.1, bf16[192,2048]{1,0:T(8,128)(2,1)} %refs_2_.1, bf16[64,3072]{1,0:T(8,128)(2,1)} %refs_3_.1, bf16[64,3072]{1,0:T(8,128)(2,1)} %refs_4_.1, ...), custom_call_target="tpu_custom_call" | custom-call | tf_op jit(solution)/shard_map/pallas_call | solution.py:658
  125.7 1.4 %shard_map.95 = (bf16[192,2048]{1,0:T(8,128)(2,1)}, bf16[192,2048]{1,0:T(8,128)(2,1)}, f32[64,3072]{1,0:T(8,128)}) custom-call(bf16[192,2048]{1,0:T(8,128)(2,1)S(1)} %get-tuple-element.6.refs_0_, bf16[192,2048]{1,0:T(8,128)(2,1)S(1)} %get-tuple-element.7.refs_1_, f32[64,3072]{1,0:T(8,128)S(1)} %get-tuple-element.8.refs_2_), custom_call_target="tpu_custom_call" | custom-call | tf_op jit(solution)/shard_map/pallas_call | solution.py:707

commit v5 on v4

--- a/solution.py
+++ b/solution.py
@@ -8,6 +8,7 @@
 from jax.sharding import PartitionSpec as P
 
 QUAD = 4
+PIECES = 1
 
 
 def contract_last(leading, trailing):
@@ -169,7 +170,7 @@
                 remote(
                     columns(weight, lane) if piece == 0 else target,
                     target,
-                    ring_ss.at[weight, way],
+                    ring_ss.at[weight],
                     first_rs.at[weight, way, 0 if piece < 2 else 1],
                     around[way],
                 )
@@ -182,7 +183,7 @@
                 remote(
                     columns(weight, relative[far]),
                     slab(weight, group, lane),
-                    quad_ss.at[weight],
+                    quad_ss.at[0],
                     quad_rs.at[weight, far - 1],
                     peers[far],
                 )
@@ -205,7 +206,7 @@
                 source,
                 row_block(token, block),
                 tok_ss.at[token],
-                tok_rs.at[token, slot],
+                tok_rs.at[token, slot % 2],
                 other,
             )
         )
@@ -242,6 +243,8 @@
     arrived = set()
 
     def arrival(weight, way, step, order):
+        if step > 1 and weight == 0:
+            weight = 1
         if (weight, way, step, order) in arrived:
             return
         arrived.add((weight, way, step, order))
@@ -251,7 +254,9 @@
             slot = first_rs.at[weight, way, side]
             remote(part, part, slot, slot, peers[1]).wait_recv()
         else:
-            hop[weight, way, step, order].wait_recv()
+            part = whole.at[0, 0 : half if weight == 2 else chunk]
+            slot = ring_rs.at[weight - 1, way, step - 2, order]
+            remote(part, part, slot, slot, peers[1]).wait_recv()
 
     def forward(weight, step, order):
         for way in range(2):
@@ -262,8 +267,8 @@
                 remote(
                     part,
                     part,
-                    ring_ss.at[weight, way],
-                    ring_rs.at[weight, way, step - 2, order],
+                    ring_ss.at[weight],
+                    ring_rs.at[max(weight - 1, 0), way, step - 2, order],
                     around[way],
                 )
             )
@@ -278,8 +283,8 @@
         send_rows(token, row_block(token, 2), 3, 2, peers[1])
 
     def token_in(token):
-        tokens[token, 0].wait_recv()
-        tokens[token, 2].wait_recv()
+        part, slot = tok.at[0, 0 : 2 * rows], tok_rs.at[token, 0]
+        remote(part, part, slot, slot, peers[1]).wait_recv()
 
     def span(owner):
         return pl.ds(pl.multiple_of(owner * chunk, chunk), chunk)
@@ -380,7 +385,7 @@
         return remote(
             near_send.at[which, owner],
             near_recv.at[which, owner],
-            near_ss.at[which],
+            near_ss.at[0],
             near_rs.at[which, owner],
             peers[1],
         )
@@ -389,8 +394,8 @@
         return remote(
             far_send.at[which, owner],
             far_recv.at[which, owner],
-            far_ss.at[which],
-            far_rs.at[which, owner],
+            far_ss.at[0],
+            far_rs.at[0 if which == 0 else 1 + lax.div(owner, 2)],
             peers[2],
         )
 
@@ -410,10 +415,20 @@
         far_copy(which, owner).start()
 
     def finish(which, owner):
-        far_copy(which, owner).wait_recv()
         outs[which][:, span(owner)] = (
             mine[which, owner, 0] + far_recv[which, owner].astype(f32)
         ).astype(bf16)
+
+    def finish_later():
+        remote(far_send.at[0], far_recv.at[0], far_ss.at[0], far_rs.at[0], peers[2]).wait_recv()
+        loop(0, ring, lambda i: finish(0, i))
+
+    def finish_pair(pair):
+        part = far_recv.at[1, pl.ds(2 * pair, 2)]
+        slot = far_rs.at[1 + pair]
+        remote(part, part, slot, slot, peers[2]).wait_recv()
+        finish(1, 2 * pair)
+        finish(1, 2 * pair + 1)
 
     last_slab = acc.shape[0] - 1
 
@@ -452,6 +467,11 @@
         else:
             slot[...] = mine_part.astype(bf16)
 
+    slots = {}
+
+    def sum_slot(*key):
+        return slots.setdefault(key, len(slots))
+
     def pass_on(way, step, order, pieces=(None,)):
         for piece in pieces:
             where = slice(None) if piece is None else piece_rows(piece)
@@ -460,8 +480,8 @@
                     remote(
                         travel.at[way, step - 1, order, where, :],
                         travel.at[way, step, order, where, :],
-                        sum_ss.at[way],
-                        sum_rs.at[way, step - 1, order, piece or 0],
+                        sum_ss.at[0],
+                        sum_rs.at[sum_slot(way, step, order, piece)],
                         around[way],
                     )
                 )
@@ -549,22 +569,20 @@
     step_piece(3, 1, 1)
     step_piece(3, 0, 0)
     relay(1, ring - 1)
-    loop(0, ring, lambda i: finish(0, i))
+    finish_later()
     step_piece(3, 0, 1)
     fold(1, 3, 1)
     pass_on(1, 3, 1)
-    loop(0, ring // 2, lambda i: finish(1, i))
+    loop(0, ring // 4, finish_pair)
     step_piece(4, 1, 0)
     step_piece(4, 1, 1)
     fold(1, 4, 0)
     pass_on(1, 4, 0, (0, 1))
-    loop(ring // 2, ring // 2 + 1, lambda i: finish(1, i))
+    finish_pair(ring // 4)
     step_piece(4, 0, 0)
     step_piece(4, 0, 1)
     fold(1, 4, 1)
     pass_on(1, 4, 1, (0, 1))
-    loop(ring // 2 + 1, ring - 1, lambda i: finish(1, i))
-
     def trade(piece, member):
         first = pl.multiple_of(member * depth, depth)
         return begin(
@@ -605,7 +623,7 @@
         trades[piece] = trade(piece, relative[piece])
 
     give(3, 1 - high, (1, 0), 0)
-    loop(ring - 1, ring, lambda i: finish(1, i))
+    loop(ring // 4 + 1, ring // 2, finish_pair)
     give(2, 1 - high, (1, 0), 1)
     give(1, high, (0, 1), 0)
     collect(3)
@@ -614,23 +632,27 @@
     collect(1)
 
     for weight in range(3):
-        settle(whole.at[weight, 0 : 3 * depth], quad_ss.at[weight])
-        for way in range(2):
-            settle(whole.at[weight, 0 : (2 * reach - 1) * half], ring_ss.at[weight, way])
+        settle(whole.at[weight, 0 : 2 * (2 * reach - 1) * half], ring_ss.at[weight])
+    settle(whole.at[0, 0 : 9 * depth], quad_ss.at[0])
     settle(tok.at[2, 0 : 3 * rows], tok_ss.at[2])
-    for index in range(2):
-        settle(near_send.at[index], near_ss.at[index])
-        settle(far_send.at[index], far_ss.at[index])
-        settle(whole.at[0, 0 : (2 * reach - 1) * half], sum_ss.at[index])
+    settle(near_send, near_ss.at[0])
+    settle(far_send, far_ss.at[0])
+    settle(whole.at[0, 0 : 2 * (2 * reach - 1) * half], sum_ss.at[0])
     settle(trade_recv, trade_ss.at[0])
 
 
 def deliver_kernel(*refs):
     sources, targets, done = refs[:3], refs[3:6], refs[6]
-    copies = [
-        pltpu.make_async_copy(source, target, done.at[index])
-        for index, (source, target) in enumerate(zip(sources, targets))
-    ]
+    copies = []
+    for index, (source, target) in enumerate(zip(sources, targets)):
+        size = source.shape[0] // PIECES
+        for piece in range(PIECES):
+            where = pl.ds(piece * size, size)
+            copies.append(
+                pltpu.make_async_copy(
+                    source.at[where, :], target.at[where, :], done.at[index, piece]
+                )
+            )
     for copy in copies:
         copy.start()
     for copy in copies:
@@ -674,19 +696,19 @@
                 pltpu.VMEM((2, reach + 1, 2, 2 * depth, width), bf16),
                 pltpu.VMEM((chunk, width), bf16),
                 pltpu.VMEM((3, depth, width), bf16),
-                dma((3,)),
+                dma((1,)),
                 dma((3, 3)),
                 dma((3, 2, 2)),
+                dma((3,)),
+                dma((2, 2, reach - 1, 2)),
+                dma((3,)),
                 dma((3, 2)),
-                dma((3, 2, reach - 1, 2)),
-                dma((3,)),
-                dma((3, 3)),
-                dma((2,)),
+                dma((1,)),
                 dma((2, ring)),
-                dma((2,)),
-                dma((2, ring)),
-                dma((2,)),
-                dma((2, reach, 2, 2)),
+                dma((1,)),
+                dma((1 + ring // 2,)),
+                dma((1,)),
+                dma((6 * reach - 1,)),
                 dma((1,)),
                 dma((3,)),
                 dma((6,)),
@@ -709,7 +731,7 @@
             out_shape=[jax.ShapeDtypeStruct(*shape) for shape in shapes],
             in_specs=[vmem] * 3,
             out_specs=[anywhere] * 3,
-            scratch_shapes=[dma((3,))],
+            scratch_shapes=[dma((3, PIECES))],
             compiler_params=pltpu.CompilerParams(vmem_limit_bytes=1_000_000),
         )(*(pltpu.with_memory_space_constraint(value, pltpu.VMEM) for value in results))
     )

time: 127 us -> 127 us (level)
  no operation moved by 1% of the time
where the time goes in v5:
time: 127 us
  Pallas kernels  126 us (99%)
    pallas_call x1, Pallas kernels, fused_shards(): pl.pallas_call(functools.partial(fused_kernel, ring, factor), out_shape=[...  125 us

profile of v5, /device:TPU:0, one launch (start us, length us, event | category | flops | bytes accessed | tf_op | source)
XLA Modules:
  0.0 126.7 jit_solution(2668027454724664571)
XLA Ops:
  0.6 124.6 %shard_map.94 = (bf16[192,2048]{1,0:T(8,128)(2,1)S(1)}, bf16[192,2048]{1,0:T(8,128)(2,1)S(1)}, f32[64,3072]{1,0:T(8,128)S(1)}) custom-call(bf16[192,2048]{1,0:T(8,128)(2,1)} %refs_0_.1, bf16[192,2048]{1,0:T(8,128)(2,1)} %refs_1_.1, bf16[192,2048]{1,0:T(8,128)(2,1)} %refs_2_.1, bf16[64,3072]{1,0:T(8,128)(2,1)} %refs_3_.1, bf16[64,3072]{1,0:T(8,128)(2,1)} %refs_4_.1, ...), custom_call_target="tpu_custom_call" | custom-call | tf_op jit(solution)/shard_map/pallas_call | solution.py:680
  125.3 1.4 %shard_map.95 = (bf16[192,2048]{1,0:T(8,128)(2,1)}, bf16[192,2048]{1,0:T(8,128)(2,1)}, f32[64,3072]{1,0:T(8,128)}) custom-call(bf16[192,2048]{1,0:T(8,128)(2,1)S(1)} %get-tuple-element.6.refs_0_, bf16[192,2048]{1,0:T(8,128)(2,1)S(1)} %get-tuple-element.7.refs_1_, f32[64,3072]{1,0:T(8,128)S(1)} %get-tuple-element.8.refs_2_), custom_call_target="tpu_custom_call" | custom-call | tf_op jit(solution)/shard_map/pallas_call | solution.py:729

commit v6 on v5

--- a/solution.py
+++ b/solution.py
@@ -170,7 +170,7 @@
                 remote(
                     columns(weight, lane) if piece == 0 else target,
                     target,
-                    ring_ss.at[weight],
+                    ring_ss.at[0],
                     first_rs.at[weight, way, 0 if piece < 2 else 1],
                     around[way],
                 )
@@ -184,7 +184,7 @@
                     columns(weight, relative[far]),
                     slab(weight, group, lane),
                     quad_ss.at[0],
-                    quad_rs.at[weight, far - 1],
+                    quad_rs.at[weight, min(far - 1, 1)],
                     peers[far],
                 )
             )
@@ -233,14 +233,23 @@
     quad[2, 1].wait_recv()
     hop_first(2, 1)
     for weight in range(3):
-        for piece in (3, 2):
-            quad[weight, piece].wait_recv()
-            hop_first(weight, piece)
+        part = half_slab(weight, group, 1 - high)
+        slot = quad_rs.at[weight, 1]
+        remote(part, part, slot, slot, peers[1]).wait_recv()
+        for way in range(2):
+            begin(
+                remote(
+                    part, part, ring_ss.at[0], first_rs.at[weight, way, 1], around[way]
+                )
+            )
     staging[3].wait()
     for part, index in ((whole.at[0, 0 : 3 * depth], 0), (tok.at[0, 0 : 3 * rows], 1)):
         pltpu.make_async_copy(part, part, local_sem.at[index]).wait()
 
     arrived = set()
+
+    def hop_slot(weight, way, step, order):
+        return (max(weight - 1, 0) * 2 + way) * (2 * reach - 3) + 2 * (step - 2) + order
 
     def arrival(weight, way, step, order):
         if step > 1 and weight == 0:
@@ -255,7 +264,7 @@
             remote(part, part, slot, slot, peers[1]).wait_recv()
         else:
             part = whole.at[0, 0 : half if weight == 2 else chunk]
-            slot = ring_rs.at[weight - 1, way, step - 2, order]
+            slot = ring_rs.at[hop_slot(weight, way, step, order)]
             remote(part, part, slot, slot, peers[1]).wait_recv()
 
     def forward(weight, step, order):
@@ -267,8 +276,8 @@
                 remote(
                     part,
                     part,
-                    ring_ss.at[weight],
-                    ring_rs.at[max(weight - 1, 0), way, step - 2, order],
+                    ring_ss.at[0],
+                    ring_rs.at[hop_slot(weight, way, step, order)],
                     around[way],
                 )
             )
@@ -631,8 +640,7 @@
     collect(2)
     collect(1)
 
-    for weight in range(3):
-        settle(whole.at[weight, 0 : 2 * (2 * reach - 1) * half], ring_ss.at[weight])
+    settle(whole.at[:, 0 : 2 * (2 * reach - 1) * half], ring_ss.at[0])
     settle(whole.at[0, 0 : 9 * depth], quad_ss.at[0])
     settle(tok.at[2, 0 : 3 * rows], tok_ss.at[2])
     settle(near_send, near_ss.at[0])
@@ -697,10 +705,10 @@
                 pltpu.VMEM((chunk, width), bf16),
                 pltpu.VMEM((3, depth, width), bf16),
                 dma((1,)),
-                dma((3, 3)),
+                dma((3, 2)),
                 dma((3, 2, 2)),
-                dma((3,)),
-                dma((2, 2, reach - 1, 2)),
+                dma((1,)),
+                dma((4 * (2 * reach - 3),)),
                 dma((3,)),
                 dma((3, 2)),
                 dma((1,)),

time: 127 us -> 127 us (level)
  no operation moved by 1% of the time
where the time goes in v6:
time: 127 us
  Pallas kernels  126 us (99%)
    pallas_call x1, Pallas kernels, fused_shards(): pl.pallas_call(functools.partial(fused_kernel, ring, factor), out_shape=[...  125 us

profile of v6, /device:TPU:0, one launch (start us, length us, event | category | flops | bytes accessed | tf_op | source)
XLA Modules:
  0.0 126.6 jit_solution(12269203881688711360)
XLA Ops:
  0.6 124.6 %shard_map.94 = (bf16[192,2048]{1,0:T(8,128)(2,1)S(1)}, bf16[192,2048]{1,0:T(8,128)(2,1)S(1)}, f32[64,3072]{1,0:T(8,128)S(1)}) custom-call(bf16[192,2048]{1,0:T(8,128)(2,1)} %refs_0_.1, bf16[192,2048]{1,0:T(8,128)(2,1)} %refs_1_.1, bf16[192,2048]{1,0:T(8,128)(2,1)} %refs_2_.1, bf16[64,3072]{1,0:T(8,128)(2,1)} %refs_3_.1, bf16[64,3072]{1,0:T(8,128)(2,1)} %refs_4_.1, ...), custom_call_target="tpu_custom_call" | custom-call | tf_op jit(solution)/shard_map/pallas_call | solution.py:688
  125.2 1.4 %shard_map.95 = (bf16[192,2048]{1,0:T(8,128)(2,1)}, bf16[192,2048]{1,0:T(8,128)(2,1)}, f32[64,3072]{1,0:T(8,128)}) custom-call(bf16[192,2048]{1,0:T(8,128)(2,1)S(1)} %get-tuple-element.6.refs_0_, bf16[192,2048]{1,0:T(8,128)(2,1)S(1)} %get-tuple-element.7.refs_1_, f32[64,3072]{1,0:T(8,128)S(1)} %get-tuple-element.8.refs_2_), custom_call_target="tpu_custom_call" | custom-call | tf_op jit(solution)/shard_map/pallas_call | solution.py:737
